TPU v7x, 512 devices: a whole 4x4x16 slice. The times are simulated.
512 devices in a mesh: ep: 16 (over y, x), tp: 32 (over z, core).
Axes of the slice: x: 4, y: 4, z: 16, core: 2. Of those that a mesh axis runs over, the one named last changes fastest.
Arguments:
- tokens: bfloat16 [3584, 4096], P('ep', 'tp'), may hold values from -6 to 6
- picks: int32 [16, 16, 56], P('ep'), may hold values from 0 to 223, as said below
- pick_weights: float32 [16, 16, 56], P('ep'), may hold values from 0.1 to 1
- gate_weight: bfloat16 [16, 1280, 4096], P('ep', 'tp'), may hold values from -0.09375 to 0.09375
- up_weight: bfloat16 [16, 1280, 4096], P('ep', 'tp'), may hold values from -0.09375 to 0.09375
- down_weight: bfloat16 [16, 1280, 4096], P('ep', None, 'tp'), may hold values from -0.15625 to 0.15625
- dense_gate: bfloat16 [5120, 4096], P('tp'), may hold values from -0.09375 to 0.09375
- dense_up: bfloat16 [5120, 4096], P('tp'), may hold values from -0.09375 to 0.09375
- dense_down: bfloat16 [5120, 4096], P('tp'), may hold values from -0.078125 to 0.078125
- branch_gate: float32 [4096], P('tp'), may hold values from -6 to 6
Outputs:
- mixed: bfloat16 [3584, 4096], P('ep', 'tp')
Inputs may be any that keep to these rules, and one draw needn't show every extreme that they name: For each block s and expert e, the 56 entries picks[s, e, :] are distinct rows of that block.
All inputs are finite; a program needn't handle non-finite values.
Results may differ from a plain program's by a relative error of at most 0.014.
Values may be sent and summed in bfloat16 or wider, within the bound.
No kernel may reach another device: no remote copies, remote signals or barrier semaphores. Data moves between devices by JAX's collectives and lax.ppermute only.
A program may use at most 64 MiB of HBM per device.

v0:
```python
import jax
import jax.numpy as jnp
from jax import lax
from jax.experimental import pallas as pl
from jax.experimental.pallas import tpu as pltpu
from jax.sharding import Mesh
from jax.sharding import PartitionSpec as P


TP = ("za", "zb", "core")
LAST = (((1,), (1,)), ((), ()))
FIRST = (((0,), (0,)), ((), ()))
PLAIN = (((1,), (0,)), ((), ()))
LANES = 128


def expert_kernel(own_ref, gate, up, down, *outs):
    own = own_ref[0]
    for k, out in enumerate(outs):
        for j in range(out.shape[2] // LANES):
            tile = j * 4 + (own ^ k)
            start = pl.multiple_of(tile * LANES, LANES)
            at = slice(j * LANES, (j + 1) * LANES)
            out[0, :, at] = gate[:, pl.ds(start, LANES)]
            out[1, :, at] = up[:, pl.ds(start, LANES)]
            out[2, :, at] = down[tile]


def dense_kernel(own_ref, gate, up, *outs):
    own = own_ref[0]
    rows = gate.shape[0]
    for k, out in enumerate(outs):
        for j in range(out.shape[1] // LANES):
            start = pl.multiple_of((j * 4 + (own ^ k)) * LANES, LANES)
            at = slice(j * LANES, (j + 1) * LANES)
            out[:rows, at] = gate[:, pl.ds(start, LANES)]
            out[rows:, at] = up[:, pl.ds(start, LANES)]


def down_kernel(own_ref, weight, *outs):
    core = own_ref[0] & 1
    for k, out in enumerate(outs):
        for j in range(out.shape[1] // LANES):
            start = pl.multiple_of((j * 2 + (core ^ k)) * LANES, LANES)
            out[:, j * LANES : (j + 1) * LANES] = weight[:, pl.ds(start, LANES)]


def split_up(kernel, own, outs, *weights):
    return pl.pallas_call(
        kernel,
        out_shape=[jax.ShapeDtypeStruct(shape, jnp.bfloat16) for shape in outs],
        in_specs=[pl.BlockSpec(memory_space=pltpu.SMEM)]
        + [pl.BlockSpec(memory_space=pltpu.VMEM)] * len(weights),
        out_specs=[pl.BlockSpec(memory_space=pltpu.VMEM)] * len(outs),
    )(own.reshape(1), *weights)


def swap(x, axes, size, k):
    return lax.ppermute(x, axes, [(i, i ^ k) for i in range(size)])


def flat(tiles):
    return jnp.moveaxis(tiles, 0, 1).reshape(tiles.shape[1], -1)


def dot(a, b, dims):
    return lax.dot_general(a, b, dims, preferred_element_type=jnp.float32)


def per_device(
    tokens,
    picks,
    pick_weights,
    gate_weight,
    up_weight,
    down_weight,
    dense_gate,
    dense_up,
    dense_down,
    branch_gate,
):
    quad = lax.axis_index("zb") * 2 + lax.axis_index("core")
    rows, width = tokens.shape
    experts, slots = picks.shape[1:]
    n_za = lax.axis_size("za")
    part = n_za * width
    hid = gate_weight.shape[1]
    dense_hid = dense_gate.shape[0]

    tiles = lax.all_to_all(
        jnp.broadcast_to(tokens, (n_za, rows, width)), "za", split_axis=0, concat_axis=0, tiled=True
    )
    mine = flat(tiles)

    down = down_weight[0].reshape(n_za * 4, hid, width)
    packs = split_up(expert_kernel, quad, [(3, hid, part)] * 4, gate_weight[0], up_weight[0], down)
    own, near, far, across = packs
    near = swap(near, "core", 2, 1)
    far = swap(far, "zb", 2, 1)
    across = swap(across, ("zb", "core"), 4, 3)
    packs = [own, near, far, across]
    gu = [x[:2].reshape(2 * hid, part) for x in packs]
    turned = jnp.stack([x[2] for x in packs]).reshape(4, hid, n_za, width)
    turned = jnp.moveaxis(turned, 2, 1).reshape(4, n_za * hid, width)
    columns = [
        lax.dynamic_index_in_dim(turned, quad ^ q, 0, keepdims=False) for q in range(4)
    ]
    down_keep, down_give = split_up(
        down_kernel, quad, [(dense_hid, 2 * part)] * 2, dense_down
    )
    down_came = swap(down_give, "core", 2, 1)
    dense_gu_weights = split_up(
        dense_kernel, quad, [(2 * dense_hid, part)] * 4, dense_gate, dense_up
    )

    chosen = picks.reshape(-1)
    pick_matrix = (
        lax.broadcasted_iota(jnp.int32, (experts * slots, rows), 1) == chosen[:, None]
    ).astype(jnp.bfloat16)
    picked = dot(pick_matrix, mine, PLAIN).astype(jnp.bfloat16)
    picked = picked.reshape(experts, slots, part)
    landed = lax.all_to_all(picked, "ep", split_axis=0, concat_axis=0, tiled=True)
    landed = landed.reshape(-1, part)

    tiles_z = swap(tiles, "zb", 2, 1)
    sets = [tiles, swap(tiles, "core", 2, 1), tiles_z, swap(tiles_z, "core", 2, 1)]
    dense_gu = sum(dot(w, flat(t), LAST) for w, t in zip(dense_gu_weights, sets))
    dense_hidden = jax.nn.silu(dense_gu[:dense_hid]) * dense_gu[dense_hid:]
    dense_hidden = dense_hidden.astype(jnp.bfloat16)
    dense_came = swap(dense_hidden, "core", 2, 1)
    wide = dot(dense_hidden, down_keep, FIRST) + dot(dense_came, down_came, FIRST)
    wide = wide.astype(jnp.bfloat16).reshape(rows, 2 * n_za, width)
    dense_out = lax.psum_scatter(
        jnp.moveaxis(wide, 1, 0), ("za", "zb"), scatter_dimension=0, tiled=False
    )

    odd = dot(jnp.concatenate([gu[1], gu[3]], 0), landed, LAST)
    odd_came = swap(odd, "core", 2, 1)
    even = dot(jnp.concatenate([gu[0], gu[2]], 0), landed, LAST) + odd_came
    far = swap(even[2 * hid :].astype(jnp.bfloat16), "zb", 2, 1)
    gate_up = even[: 2 * hid] + far.astype(jnp.float32)
    hidden = (jax.nn.silu(gate_up[:hid]) * gate_up[hid:]).astype(jnp.bfloat16)

    units = lax.all_gather(hidden, "za", axis=0, tiled=True)
    outgoing = jnp.stack([dot(units, c, FIRST).astype(jnp.bfloat16) for c in columns])
    outgoing = outgoing.reshape(4 * experts, slots, width)
    back = lax.all_to_all(outgoing, ("zb", "core", "ep"), split_axis=0, concat_axis=0, tiled=True)

    token = lax.broadcasted_iota(jnp.int32, (rows, experts * slots), 0)
    spread = jnp.where(token == chosen[None, :], pick_weights.reshape(1, -1), 0.0)
    spread = jnp.tile(spread.astype(jnp.bfloat16), (1, 4))
    mixture = dot(spread, back.reshape(4 * experts * slots, width), PLAIN)
    mixed = mixture + jax.nn.sigmoid(branch_gate)[None, :] * dense_out.astype(jnp.float32)
    return mixed.astype(jnp.bfloat16)


def solution(mesh):
    split = Mesh(
        mesh.devices.reshape(mesh.shape["ep"], mesh.shape["tp"] // 4, 2, 2),
        ("ep", "za", "zb", "core"),
    )
    placed = (
        P("ep", TP),
        P("ep", None, None),
        P("ep", None, None),
        P("ep", TP, None),
        P("ep", TP, None),
        P("ep", None, TP),
        P(TP, None),
        P(TP, None),
        P(TP, None),
        P(TP),
    )

    return jax.shard_map(
        per_device, mesh=split, in_specs=placed, out_specs=P("ep", TP), check_vma=False
    )
```

profile of v0, /device:TPU:2, one launch (start us, length us, event | category | flops | bytes accessed | tf_op | source)
XLA Modules:
  0.0 255.5 jit_solution(3268282785646860577)
XLA Ops:
  6.5 1.7 broadcast_in_dim.21
  8.2 15.1 %all-to-all-start = ((bf16[8,224,128]{2,1,0:T(8,128)(2,1)}), bf16[8,224,128]{2,1,0:T(8,128)(2,1)S(1)}, u32[]{:S(2)}, u32[]{:S(2)}) async-start(bf16[8,224,128]{2,1,0:T(8,128)(2,1)} %broadcast_in_dim.21), calls=%async_computation | async-start | bytes 917504 | tf_op jit(solution)/shard_map/all_to_all | solution.py:90
  24.1 24.3 %all-to-all-done = bf16[8,224,128]{2,1,0:T(8,128)(2,1)S(1)} async-done(((bf16[8,224,128]{2,1,0:T(8,128)(2,1)}), bf16[8,224,128]{2,1,0:T(8,128)(2,1)S(1)}, u32[]{:S(2)}, u32[]{:S(2)}) %all-to-all-start) | async-done | bytes 458784 | tf_op jit(solution)/shard_map/all_to_all | solution.py:90
  48.4 1.9 convolution_convert_fusion
  50.3 7.5 %all-to-all-start.1 = ((bf16[16,56,1024]{2,1,0:T(8,128)(2,1)}), bf16[16,56,1024]{2,1,0:T(8,128)(2,1)S(1)}, u32[]{:S(2)}, u32[]{:S(2)}) async-start(bf16[16,56,1024]{2,1,0:T(8,128)(2,1)} %bitcast.108), calls=%async_computation.1 | async-start | bytes 3670016 | tf_op jit(solution)/shard_map/all_to_all | solution.py:122
  57.8 2.3 shard_map.100
  60.1 2.0 collective-permute-start.2
  62.2 4.6 %collective-permute-start.1 = (bf16[3,40,1024]{2,1,0:T(8,128)(2,1)}, bf16[3,40,1024]{2,1,0:T(8,128)(2,1)S(1)}, u32[]{:S(2)}, u32[]{:S(2)}) collective-permute-start(bf16[3,40,1024]{2,1,0:T(8,128)(2,1)} %get-tuple-element.17), channel_id=1, source_target_pairs={{0,1},{1,0},{2,3},{3,2},{4,5},{5,4},{6,7},{7,6},{8,9},{9,8},{10,11... | collective-permute-start | bytes 737288 | tf_op jit(solution)/shard_map/ppermute | solution.py:59
  66.8 2.7 %collective-permute-done.2 = bf16[3,40,1024]{2,1,0:T(8,128)(2,1)S(1)} collective-permute-done((bf16[3,40,1024]{2,1,0:T(8,128)(2,1)}, bf16[3,40,1024]{2,1,0:T(8,128)(2,1)S(1)}, u32[]{:S(2)}, u32[]{:S(2)}) %collective-permute-start.2) | collective-permute-done | bytes 245792 | tf_op jit(solution)/shard_map/ppermute | solution.py:59
  69.5 11.2 %all-to-all-done.1 = bf16[16,56,1024]{2,1,0:T(8,128)(2,1)S(1)} async-done(((bf16[16,56,1024]{2,1,0:T(8,128)(2,1)}), bf16[16,56,1024]{2,1,0:T(8,128)(2,1)S(1)}, u32[]{:S(2)}, u32[]{:S(2)}) %all-to-all-start.1) | async-done | bytes 1835040 | tf_op jit(solution)/shard_map/all_to_all | solution.py:122
  81.5 1.9 collective-permute-start.3
  83.4 3.9 %collective-permute-start = (bf16[3,40,1024]{2,1,0:T(8,128)(2,1)S(1)}, bf16[3,40,1024]{2,1,0:T(8,128)(2,1)S(1)}, u32[]{:S(2)}, u32[]{:S(2)}) collective-permute-start(bf16[3,40,1024]{2,1,0:T(8,128)(2,1)S(1)} %copy-done.7), channel_id=1, source_target_pairs={{0,2},{2,0},{1,3},{3,1},{4,6},{6,4},{5,7},{7,5},{8,10},{10,8},{9,1... | collective-permute-start | bytes 737288 | tf_op jit(solution)/shard_map/ppermute | solution.py:59
  87.4 6.6 %collective-permute-done = bf16[3,40,1024]{2,1,0:T(8,128)(2,1)S(1)} collective-permute-done((bf16[3,40,1024]{2,1,0:T(8,128)(2,1)S(1)}, bf16[3,40,1024]{2,1,0:T(8,128)(2,1)S(1)}, u32[]{:S(2)}, u32[]{:S(2)}) %collective-permute-start) | collective-permute-done | bytes 245792 | tf_op jit(solution)/shard_map/ppermute | solution.py:59
  95.4 3.6 %collective-permute-start.4 = (bf16[80,896]{1,0:T(8,128)(2,1)S(1)}, bf16[80,896]{1,0:T(8,128)(2,1)S(1)}, u32[]{:S(2)}, u32[]{:S(2)}) collective-permute-start(bf16[80,896]{1,0:T(8,128)(2,1)S(1)} %slice.79), channel_id=1, source_target_pairs={{0,2},{2,0},{1,3},{3,1},{4,6},{6,4},{5,7},{7,5},{8,10},{10,8},{9,1... | collective-permute-start | bytes 430088 | tf_op jit(solution)/shard_map/ppermute | solution.py:59
  99.1 2.7 %shard_map.102 = (bf16[160,2048]{1,0:T(8,128)(2,1)}, bf16[160,2048]{1,0:T(8,128)(2,1)}) custom-call(s32[1]{0:T(128)} %bitcast.own_ref, bf16[160,4096]{1,0:T(8,128)(2,1)} %weight.1), custom_call_target="tpu_custom_call" | custom-call | tf_op jit(solution)/shard_map/pallas_call | solution.py:49
  101.8 1.9 collective-permute-start.9
  103.7 0.9 slice.51
  104.6 3.9 %shard_map.101 = (bf16[320,1024]{1,0:T(8,128)(2,1)}, bf16[320,1024]{1,0:T(8,128)(2,1)}, bf16[320,1024]{1,0:T(8,128)(2,1)}, bf16[320,1024]{1,0:T(8,128)(2,1)}) custom-call(s32[1]{0:T(128)} %bitcast.own_ref, bf16[160,4096]{1,0:T(8,128)(2,1)} %gate.1, bf16[160,4096]{1,0:T(8,128)(2,1)} %up.1), custom_call_target="tpu_custom_call" | custom-call | tf_op jit(solution)/shard_map/pallas_call | solution.py:49
  108.6 0.9 slice.65
  109.5 2.4 collective-permute-start.5
  112.0 2.2 collective-permute-start.6
  114.3 42.1 %all_gather.3 = bf16[320,896]{1,0:T(8,128)(2,1)S(1)} all-gather(bf16[40,896]{1,0:T(8,128)(2,1)S(1)} %fusion.27), channel_id=1, replica_groups=mesh['ep'=16,'za'=8,'zb'=2,'core'=2] {'za'}, dimensions={0}, use_global_device_ids=true | all-gather | bytes 645120 | tf_op jit(solution)/shard_map/all_gather | solution.py:144
  157.9 1.1 pad_maximum_fusion
  159.0 7.5 %all-to-all-start.2 = ((bf16[64,56,128]{2,1,0:T(8,128)(2,1)}), bf16[64,56,128]{2,1,0:T(8,128)(2,1)S(1)}, u32[]{:S(2)}, u32[]{:S(2)}) async-start(bf16[64,56,128]{2,1,0:T(8,128)(2,1)} %bitcast.22), calls=%async_computation.2 | async-start | bytes 1835008 | tf_op jit(solution)/shard_map/all_to_all | solution.py:147
  166.5 1.5 fusion.13
  168.0 2.3 collective-permute-start.7
  170.3 1.4 convolution_add_fusion.4
  172.6 2.2 collective-permute-start.8
  175.7 1.5 fusion.1
  177.3 1.1 copy.48
  179.7 66.9 %reduce-scatter.2.cloned.1.call-done = bf16[1,224,128]{2,1,0:T(8,128)(2,1)} async-done(((bf16[16,224,128]{2,1,0:T(8,128)(2,1)}), bf16[1,224,128]{2,1,0:T(8,128)(2,1)}) %reduce-scatter.2.cloned.1.call-update) | async-done | bytes 57360 | tf_op jit(solution)/shard_map/reduce_scatter | solution.py:133
  246.6 2.0 fusion.6
  (55 shorter events, 7.8 us)
Async XLA Ops:
  8.2 40.1 %all-to-all-start = ((bf16[8,224,128]{2,1,0:T(8,128)(2,1)}), bf16[8,224,128]{2,1,0:T(8,128)(2,1)S(1)}, u32[]{:S(2)}, u32[]{:S(2)}) async-start(bf16[8,224,128]{2,1,0:T(8,128)(2,1)} %broadcast_in_dim.21), calls=%async_computation | async-start | bytes 917504 | tf_op jit(solution)/shard_map/all_to_all | solution.py:90
  50.3 30.4 %all-to-all-start.1 = ((bf16[16,56,1024]{2,1,0:T(8,128)(2,1)}), bf16[16,56,1024]{2,1,0:T(8,128)(2,1)S(1)}, u32[]{:S(2)}, u32[]{:S(2)}) async-start(bf16[16,56,1024]{2,1,0:T(8,128)(2,1)} %bitcast.108), calls=%async_computation.1 | async-start | bytes 3670016 | tf_op jit(solution)/shard_map/all_to_all | solution.py:122
  60.1 27.2 %copy-start.5 = (bf16[3,40,1024]{2,1,0:T(8,128)(2,1)S(1)}, bf16[3,40,1024]{2,1,0:T(8,128)(2,1)}, u32[]{:S(2)}) copy-start(bf16[3,40,1024]{2,1,0:T(8,128)(2,1)} %get-tuple-element.15) | copy-start | bytes 737284
  60.1 9.3 %collective-permute-start.2 = (bf16[3,40,1024]{2,1,0:T(8,128)(2,1)}, bf16[3,40,1024]{2,1,0:T(8,128)(2,1)S(1)}, u32[]{:S(2)}, u32[]{:S(2)}) collective-permute-start(bf16[3,40,1024]{2,1,0:T(8,128)(2,1)} %get-tuple-element.18), channel_id=1, source_target_pairs={{0,3},{1,2},{2,1},{3,0},{4,7},{5,6},{6,5},{7,4},{8,11},{9,10},{10,... | collective-permute-start | bytes 737288 | tf_op jit(solution)/shard_map/ppermute | solution.py:59
  62.2 7.3 %collective-permute-start.1 = (bf16[3,40,1024]{2,1,0:T(8,128)(2,1)}, bf16[3,40,1024]{2,1,0:T(8,128)(2,1)S(1)}, u32[]{:S(2)}, u32[]{:S(2)}) collective-permute-start(bf16[3,40,1024]{2,1,0:T(8,128)(2,1)} %get-tuple-element.17), channel_id=1, source_target_pairs={{0,1},{1,0},{2,3},{3,2},{4,5},{5,4},{6,7},{7,6},{8,9},{9,8},{10,11... | collective-permute-start | bytes 737288 | tf_op jit(solution)/shard_map/ppermute | solution.py:59
  80.7 2.7 %copy-start.7 = (bf16[3,40,1024]{2,1,0:T(8,128)(2,1)S(1)}, bf16[3,40,1024]{2,1,0:T(8,128)(2,1)}, u32[]{:S(2)}) copy-start(bf16[3,40,1024]{2,1,0:T(8,128)(2,1)} %get-tuple-element.16) | copy-start | bytes 737284
  81.5 12.5 %collective-permute-start.3 = (f32[160,896]{1,0:T(8,128)S(1)}, f32[160,896]{1,0:T(8,128)S(1)}, u32[]{:S(2)}, u32[]{:S(2)}) collective-permute-start(f32[160,896]{1,0:T(8,128)S(1)} %fusion.22), channel_id=1, source_target_pairs={{0,1},{1,0},{2,3},{3,2},{4,5},{5,4},{6,7},{7,6},{8,9},{9,8},{10,11... | collective-permute-start | bytes 1720328 | tf_op jit(solution)/shard_map/ppermute | solution.py:59
  83.4 10.6 %collective-permute-start = (bf16[3,40,1024]{2,1,0:T(8,128)(2,1)S(1)}, bf16[3,40,1024]{2,1,0:T(8,128)(2,1)S(1)}, u32[]{:S(2)}, u32[]{:S(2)}) collective-permute-start(bf16[3,40,1024]{2,1,0:T(8,128)(2,1)S(1)} %copy-done.7), channel_id=1, source_target_pairs={{0,2},{2,0},{1,3},{3,1},{4,6},{6,4},{5,7},{7,5},{8,10},{10,8},{9,1... | collective-permute-start | bytes 737288 | tf_op jit(solution)/shard_map/ppermute | solution.py:59
  94.0 0.7 copy-start.4
  95.4 18.7 %collective-permute-start.4 = (bf16[80,896]{1,0:T(8,128)(2,1)S(1)}, bf16[80,896]{1,0:T(8,128)(2,1)S(1)}, u32[]{:S(2)}, u32[]{:S(2)}) collective-permute-start(bf16[80,896]{1,0:T(8,128)(2,1)S(1)} %slice.79), channel_id=1, source_target_pairs={{0,2},{2,0},{1,3},{3,1},{4,6},{6,4},{5,7},{7,5},{8,10},{10,8},{9,1... | collective-permute-start | bytes 430088 | tf_op jit(solution)/shard_map/ppermute | solution.py:59
  101.8 73.4 %collective-permute-start.9 = (bf16[160,2048]{1,0:T(8,128)(2,1)}, bf16[160,2048]{1,0:T(8,128)(2,1)}, u32[]{:S(2)}, u32[]{:S(2)}) collective-permute-start(bf16[160,2048]{1,0:T(8,128)(2,1)} %get-tuple-element.24), channel_id=1, source_target_pairs={{0,1},{1,0},{2,3},{3,2},{4,5},{5,4},{6,7},{7,6},{8,9},{9,8},{10,11... | collective-permute-start | bytes 1966088 | tf_op jit(solution)/shard_map/ppermute | solution.py:59
  109.5 60.8 %collective-permute-start.5 = (bf16[8,224,128]{2,1,0:T(8,128)(2,1)S(1)}, bf16[8,224,128]{2,1,0:T(8,128)(2,1)}, u32[]{:S(2)}, u32[]{:S(2)}) collective-permute-start(bf16[8,224,128]{2,1,0:T(8,128)(2,1)S(1)} %all-to-all-done), channel_id=1, source_target_pairs={{0,1},{1,0},{2,3},{3,2},{4,5},{5,4},{6,7},{7,6},{8,9},{9,8},{10,11... | collective-permute-start | bytes 1376264 | tf_op jit(solution)/shard_map/ppermute | solution.py:59
  112.0 56.1 %collective-permute-start.6 = (bf16[8,224,128]{2,1,0:T(8,128)(2,1)S(1)}, bf16[8,224,128]{2,1,0:T(8,128)(2,1)S(1)}, u32[]{:S(2)}, u32[]{:S(2)}) collective-permute-start(bf16[8,224,128]{2,1,0:T(8,128)(2,1)S(1)} %all-to-all-done), channel_id=1, source_target_pairs={{0,2},{2,0},{1,3},{3,1},{4,6},{6,4},{5,7},{7,5},{8,10},{10,8},{9,1... | collective-permute-start | bytes 1376264 | tf_op jit(solution)/shard_map/ppermute | solution.py:59
  159.0 11.4 %copy-start.3 = (bf16[320,1024]{1,0:T(8,128)(2,1)S(1)}, bf16[320,1024]{1,0:T(8,128)(2,1)}, u32[]{:S(2)}) copy-start(bf16[320,1024]{1,0:T(8,128)(2,1)} %get-tuple-element.20) | copy-start | bytes 1966084
  159.0 87.6 %all-to-all-start.2 = ((bf16[64,56,128]{2,1,0:T(8,128)(2,1)}), bf16[64,56,128]{2,1,0:T(8,128)(2,1)S(1)}, u32[]{:S(2)}, u32[]{:S(2)}) async-start(bf16[64,56,128]{2,1,0:T(8,128)(2,1)} %bitcast.22), calls=%async_computation.2 | async-start | bytes 1835008 | tf_op jit(solution)/shard_map/all_to_all | solution.py:147
  166.4 5.3 %copy-start.2 = (bf16[320,1024]{1,0:T(8,128)(2,1)S(1)}, bf16[320,1024]{1,0:T(8,128)(2,1)}, u32[]{:S(2)}) copy-start(bf16[320,1024]{1,0:T(8,128)(2,1)} %get-tuple-element.21) | copy-start | bytes 1966084
  166.5 80.2 %reduce-scatter.2.cloned.1.call-start = ((), (), s32[]{:S(2)}) async-start(), calls=%async_computation.4 | async-start | bytes 974848 | tf_op jit(solution)/shard_map/reduce_scatter | solution.py:133
  168.0 4.1 %copy-start.1 = (bf16[320,1024]{1,0:T(8,128)(2,1)S(1)}, bf16[320,1024]{1,0:T(8,128)(2,1)}, u32[]{:S(2)}) copy-start(bf16[320,1024]{1,0:T(8,128)(2,1)} %get-tuple-element.22) | copy-start | bytes 1966084
  168.0 4.1 %collective-permute-start.7 = (bf16[8,224,128]{2,1,0:T(8,128)(2,1)S(1)}, bf16[8,224,128]{2,1,0:T(8,128)(2,1)S(1)}, u32[]{:S(2)}, u32[]{:S(2)}) collective-permute-start(bf16[8,224,128]{2,1,0:T(8,128)(2,1)S(1)} %collective-permute-done.6), channel_id=1, source_target_pairs={{0,1},{1,0},{2,3},{3,2},{4,5},{5,4},{6,7},{7,6},{8,9},{9,8},{10,11... | collective-permute-start | bytes 1376264 | tf_op jit(solution)/shard_map/ppermute | solution.py:59
  171.7 3.0 %copy-start = (bf16[160,2048]{1,0:T(8,128)(2,1)S(1)}, bf16[160,2048]{1,0:T(8,128)(2,1)}, u32[]{:S(2)}) copy-start(bf16[160,2048]{1,0:T(8,128)(2,1)} %get-tuple-element.23) | copy-start | bytes 1966084
  172.6 3.2 %collective-permute-start.8 = (bf16[160,224]{1,0:T(8,128)(2,1)S(1)}, bf16[160,224]{1,0:T(8,128)(2,1)S(1)}, u32[]{:S(2)}, u32[]{:S(2)}) collective-permute-start(bf16[160,224]{1,0:T(8,128)(2,1)S(1)} %fusion.26), channel_id=1, source_target_pairs={{0,1},{1,0},{2,3},{3,2},{4,5},{5,4},{6,7},{7,6},{8,9},{9,8},{10,11... | collective-permute-start | bytes 215048 | tf_op jit(solution)/shard_map/ppermute | solution.py:59
  177.2 1.1 copy-start.6
  179.0 0.7 copy-start.8
Sparse Core Ops, SparseCore 0:
  178.5 68.0 reduce-scatter.1
where the time goes:
time: 257 us; the launch traced here: 255 us
  waiting for transfers between devices  112 us (44%)
  starting transfers between devices  57.2 us (22%)
  blocking collectives  42.1 us (16%)
  between operations  13.8 us (5%)
  matrix products  12.5 us (5%)
  Pallas kernels  9 us (4%)
  local copies, waits for them, and re-layouts  7.25 us (3%)
    reduce_scatter x1, waiting for transfers between devices, per_device(): lax.psum_scatter(jnp.moveaxis(wide, 1, 0), ('za', 'zb'), scatter_dimensio...  66.9 us
    all_gather x1, blocking collectives, per_device(): units = lax.all_gather(hidden, 'za', axis=0, tiled=True)  42.1 us
    ppermute x10, starting transfers between devices, swap(): return lax.ppermute(x, axes, [(i, i ^ k) for i in range(size)])  27.1 us
    all_to_all x1, waiting for transfers between devices, per_device(): lax.all_to_all(jnp.broadcast_to(tokens, (n_za, rows, width)), 'za', split...  24.3 us
    all_to_all x1, starting transfers between devices, per_device(): lax.all_to_all(jnp.broadcast_to(tokens, (n_za, rows, width)), 'za', split...  15.1 us
    dot_general x14, matrix products, dot(): return lax.dot_general(a, b, dims, preferred_element_type=jnp.float32)  12.5 us
    all_to_all x1, waiting for transfers between devices, per_device(): lax.all_to_all(picked, 'ep', split_axis=0, concat_axis=0, tiled=True)  11.2 us
    ppermute x10, waiting for transfers between devices, swap(): return lax.ppermute(x, axes, [(i, i ^ k) for i in range(size)])  9.77 us
  transfers between devices with their start and end apart: 14, of which 6 were waited for; matrix products, arithmetic and copies ran while one was open for 5% of the time, Pallas kernels for 4%

commit v1 on v0

--- a/solution.py
+++ b/solution.py
@@ -14,27 +14,30 @@
 LANES = 128
 
 
-def expert_kernel(own_ref, gate, up, down, *outs):
+def expert_kernel(own_ref, gate, up, down, gu_own, gu_far, gu_near, own_out, far_out, near_out):
     own = own_ref[0]
-    for k, out in enumerate(outs):
-        for j in range(out.shape[2] // LANES):
+    pairs = (gu_own, gu_near.at[0], gu_far, gu_near.at[1])
+    turns = (own_out, near_out.at[0], far_out, near_out.at[1])
+    for k in range(4):
+        for j in range(own_out.shape[0]):
             tile = j * 4 + (own ^ k)
             start = pl.multiple_of(tile * LANES, LANES)
             at = slice(j * LANES, (j + 1) * LANES)
-            out[0, :, at] = gate[:, pl.ds(start, LANES)]
-            out[1, :, at] = up[:, pl.ds(start, LANES)]
-            out[2, :, at] = down[tile]
+            pairs[k][0, :, at] = gate[:, pl.ds(start, LANES)]
+            pairs[k][1, :, at] = up[:, pl.ds(start, LANES)]
+            turns[k][j] = down[tile]
 
 
-def dense_kernel(own_ref, gate, up, *outs):
+def dense_kernel(own_ref, gate, up, keep, give):
     own = own_ref[0]
     rows = gate.shape[0]
-    for k, out in enumerate(outs):
-        for j in range(out.shape[1] // LANES):
+    for k in range(4):
+        out = give if k % 2 else keep
+        for j in range(out.shape[2] // LANES):
             start = pl.multiple_of((j * 4 + (own ^ k)) * LANES, LANES)
             at = slice(j * LANES, (j + 1) * LANES)
-            out[:rows, at] = gate[:, pl.ds(start, LANES)]
-            out[rows:, at] = up[:, pl.ds(start, LANES)]
+            out[k // 2, :rows, at] = gate[:, pl.ds(start, LANES)]
+            out[k // 2, rows:, at] = up[:, pl.ds(start, LANES)]
 
 
 def down_kernel(own_ref, weight, *outs):
@@ -93,25 +96,35 @@
     mine = flat(tiles)
 
     down = down_weight[0].reshape(n_za * 4, hid, width)
-    packs = split_up(expert_kernel, quad, [(3, hid, part)] * 4, gate_weight[0], up_weight[0], down)
-    own, near, far, across = packs
-    near = swap(near, "core", 2, 1)
-    far = swap(far, "zb", 2, 1)
-    across = swap(across, ("zb", "core"), 4, 3)
-    packs = [own, near, far, across]
-    gu = [x[:2].reshape(2 * hid, part) for x in packs]
-    turned = jnp.stack([x[2] for x in packs]).reshape(4, hid, n_za, width)
-    turned = jnp.moveaxis(turned, 2, 1).reshape(4, n_za * hid, width)
+    pair, turn = (2, hid, part), (n_za, hid, width)
+    gu_own, gu_far, gu_near, turn_own, turn_far, turn_near = split_up(
+        expert_kernel,
+        quad,
+        [pair, pair, (2, *pair), turn, turn, (2, *turn)],
+        gate_weight[0],
+        up_weight[0],
+        down,
+    )
+    gu_near = swap(gu_near, "core", 2, 1)
+    relay = jnp.stack([gu_far, gu_near[1]])
+    gu_far = swap(relay, "zb", 2, 1)
+    gu = [gu_own, gu_near[0], gu_far[0], gu_far[1]]
+    gu = [x.reshape(2 * hid, part) for x in gu]
+    turn_near = swap(turn_near, "core", 2, 1)
+    turn_far = swap(jnp.stack([turn_far, turn_near[1]]), "zb", 2, 1)
+    turned = jnp.stack([turn_own, turn_near[0], turn_far[0], turn_far[1]])
+    turned = turned.reshape(4, n_za * hid, width)
     columns = [
         lax.dynamic_index_in_dim(turned, quad ^ q, 0, keepdims=False) for q in range(4)
     ]
+    dense_keep, dense_give = split_up(
+        dense_kernel, quad, [(2, 2 * dense_hid, part)] * 2, dense_gate, dense_up
+    )
     down_keep, down_give = split_up(
         down_kernel, quad, [(dense_hid, 2 * part)] * 2, dense_down
     )
+    dense_came = swap(dense_give, "core", 2, 1)
     down_came = swap(down_give, "core", 2, 1)
-    dense_gu_weights = split_up(
-        dense_kernel, quad, [(2 * dense_hid, part)] * 4, dense_gate, dense_up
-    )
 
     chosen = picks.reshape(-1)
     pick_matrix = (
@@ -122,13 +135,19 @@
     landed = lax.all_to_all(picked, "ep", split_axis=0, concat_axis=0, tiled=True)
     landed = landed.reshape(-1, part)
 
-    tiles_z = swap(tiles, "zb", 2, 1)
-    sets = [tiles, swap(tiles, "core", 2, 1), tiles_z, swap(tiles_z, "core", 2, 1)]
-    dense_gu = sum(dot(w, flat(t), LAST) for w, t in zip(dense_gu_weights, sets))
-    dense_hidden = jax.nn.silu(dense_gu[:dense_hid]) * dense_gu[dense_hid:]
-    dense_hidden = dense_hidden.astype(jnp.bfloat16)
-    dense_came = swap(dense_hidden, "core", 2, 1)
-    wide = dot(dense_hidden, down_keep, FIRST) + dot(dense_came, down_came, FIRST)
+    tiles_far = swap(tiles, "zb", 2, 1)
+    firsts = [dot(w[0], mine, LAST) for w in (dense_keep, dense_came)]
+    firsts = lax.optimization_barrier(firsts)
+    theirs = flat(tiles_far)
+    own_part, pair_part = (
+        first + dot(w[1], theirs, LAST) for first, w in zip(firsts, (dense_keep, dense_came))
+    )
+    came_part = swap(jnp.stack([pair_part, own_part]), "core", 2, 1)
+    dense_hidden = []
+    for gu_sum in (own_part + came_part[0], pair_part + came_part[1]):
+        value = jax.nn.silu(gu_sum[:dense_hid]) * gu_sum[dense_hid:]
+        dense_hidden.append(value.astype(jnp.bfloat16))
+    wide = dot(dense_hidden[0], down_keep, FIRST) + dot(dense_hidden[1], down_came, FIRST)
     wide = wide.astype(jnp.bfloat16).reshape(rows, 2 * n_za, width)
     dense_out = lax.psum_scatter(
         jnp.moveaxis(wide, 1, 0), ("za", "zb"), scatter_dimension=0, tiled=False

time: 257 us -> 247 us (0.961)
  waiting for transfers between devices: 112 us -> 106 us
    all_to_all x1, waiting for transfers between devices: 11.2 us -> 0.01 us  [per_device(): lax.all_to_all(picked, 'ep', split_axis=0, concat_axis=0, tiled=True)]
    ppermute x10, waiting for transfers between devices: 9.77 us -> 15 us  [swap(): return lax.ppermute(x, axes, [(i, i ^ k) for i in range(size)])]
  transfers between devices with their start and end apart: 14 -> 14, of which waited for: 6 -> 6; matrix products, arithmetic and copies ran while one was open for 5% -> 6% of each run, Pallas kernels for 4% -> 4%
where the time goes in v1:
time: 247 us; the launch traced here: 246 us
  waiting for transfers between devices  106 us (43%)
  starting transfers between devices  57.3 us (23%)
  blocking collectives  39.8 us (16%)
  matrix products  13.8 us (6%)
  between operations  13.8 us (6%)
  Pallas kernels  8.99 us (4%)
  local copies, waits for them, and re-layouts  4.8 us (2%)
    reduce_scatter x1, waiting for transfers between devices, per_device(): lax.psum_scatter(jnp.moveaxis(wide, 1, 0), ('za', 'zb'), scatter_dimensio...  66.4 us
    all_gather x1, blocking collectives, per_device(): units = lax.all_gather(hidden, 'za', axis=0, tiled=True)  39.8 us
    ppermute x10, starting transfers between devices, swap(): return lax.ppermute(x, axes, [(i, i ^ k) for i in range(size)])  26.8 us
    all_to_all x1, waiting for transfers between devices, per_device(): lax.all_to_all(jnp.broadcast_to(tokens, (n_za, rows, width)), 'za', split...  24.3 us
    all_to_all x1, starting transfers between devices, per_device(): lax.all_to_all(jnp.broadcast_to(tokens, (n_za, rows, width)), 'za', split...  15.1 us
    ppermute x10, waiting for transfers between devices, swap(): return lax.ppermute(x, axes, [(i, i ^ k) for i in range(size)])  15 us
    dot_general x14, matrix products, dot(): return lax.dot_general(a, b, dims, preferred_element_type=jnp.float32)  13.8 us
    pallas_call x3, Pallas kernels, split_up(): pl.pallas_call(kernel, out_shape=[jax.ShapeDtypeStruct(shape, jnp.bfloat1...  8.99 us
  transfers between devices with their start and end apart: 14, of which 6 were waited for; matrix products, arithmetic and copies ran while one was open for 6% of the time, Pallas kernels for 4%

profile of v1, /device:TPU:2, one launch (start us, length us, event | category | flops | bytes accessed | tf_op | source)
XLA Modules:
  0.0 246.3 jit_solution(11729173439005434731)
XLA Ops:
  6.5 1.7 broadcast_in_dim.21
  8.2 15.1 %all-to-all-start = ((bf16[8,224,128]{2,1,0:T(8,128)(2,1)}), bf16[8,224,128]{2,1,0:T(8,128)(2,1)S(1)}, u32[]{:S(2)}, u32[]{:S(2)}) async-start(bf16[8,224,128]{2,1,0:T(8,128)(2,1)} %broadcast_in_dim.21), calls=%async_computation | async-start | bytes 917504 | tf_op jit(solution)/shard_map/all_to_all | solution.py:93
  23.3 0.8 eq.22
  24.1 24.3 %all-to-all-done = bf16[8,224,128]{2,1,0:T(8,128)(2,1)S(1)} async-done(((bf16[8,224,128]{2,1,0:T(8,128)(2,1)}), bf16[8,224,128]{2,1,0:T(8,128)(2,1)S(1)}, u32[]{:S(2)}, u32[]{:S(2)}) %all-to-all-start) | async-done | bytes 458784 | tf_op jit(solution)/shard_map/all_to_all | solution.py:93
  48.3 1.9 convolution_convert_fusion
  50.3 7.5 %all-to-all-start.1 = ((bf16[16,56,1024]{2,1,0:T(8,128)(2,1)}), bf16[16,56,1024]{2,1,0:T(8,128)(2,1)S(1)}, u32[]{:S(2)}, u32[]{:S(2)}) async-start(bf16[16,56,1024]{2,1,0:T(8,128)(2,1)} %bitcast.115), calls=%async_computation.1 | async-start | bytes 3670016 | tf_op jit(solution)/shard_map/all_to_all | solution.py:135
  57.8 2.4 shard_map.100
  60.1 2.0 collective-permute-start
  62.2 3.9 %shard_map.101 = (bf16[2,320,1024]{2,1,0:T(8,128)(2,1)}, bf16[2,320,1024]{2,1,0:T(8,128)(2,1)}) custom-call(s32[1]{0:T(128)} %bitcast.own_ref, bf16[160,4096]{1,0:T(8,128)(2,1)} %gate.1, bf16[160,4096]{1,0:T(8,128)(2,1)} %up.1), custom_call_target="tpu_custom_call" | custom-call | tf_op jit(solution)/shard_map/pallas_call | solution.py:52
  66.1 2.4 collective-permute-start.6
  68.5 1.9 collective-permute-start.4
  70.5 4.5 %collective-permute-start.1 = (bf16[2,2,40,1024]{3,2,1,0:T(8,128)(2,1)S(1)}, bf16[2,2,40,1024]{3,2,1,0:T(8,128)(2,1)S(1)}, u32[]{:S(2)}, u32[]{:S(2)}) collective-permute-start(bf16[2,2,40,1024]{3,2,1,0:T(8,128)(2,1)S(1)} %pad_maximum_fusion.2), channel_id=1, source_target_pairs={{0,2},{2,0},{1,3},{3,1},{4,6},{6,4},{5,7},{7,5},{8,10},{10,8},{9,1... | collective-permute-start | bytes 983048 | tf_op jit(solution)/shard_map/ppermute | solution.py:62
  75.1 8.3 %collective-permute-done.1 = bf16[2,2,40,1024]{3,2,1,0:T(8,128)(2,1)S(1)} collective-permute-done((bf16[2,2,40,1024]{3,2,1,0:T(8,128)(2,1)S(1)}, bf16[2,2,40,1024]{3,2,1,0:T(8,128)(2,1)S(1)}, u32[]{:S(2)}, u32[]{:S(2)}) %collective-permute-start.1) | collective-permute-done | bytes 327712 | tf_op jit(solution)/shard_map/ppermute | solution.py:62
  83.4 1.6 fusion.29
  85.0 2.0 collective-permute-start.2
  87.7 3.6 %collective-permute-start.5 = (bf16[2,8,40,128]{3,2,1,0:T(8,128)(2,1)}, bf16[2,8,40,128]{3,2,1,0:T(8,128)(2,1)S(1)}, u32[]{:S(2)}, u32[]{:S(2)}) collective-permute-start(bf16[2,8,40,128]{3,2,1,0:T(8,128)(2,1)} %pad_maximum_fusion.4), channel_id=1, source_target_pairs={{0,2},{2,0},{1,3},{3,1},{4,6},{6,4},{5,7},{7,5},{8,10},{10,8},{9,1... | collective-permute-start | bytes 491528 | tf_op jit(solution)/shard_map/ppermute | solution.py:62
  91.4 5.0 %collective-permute-done.5 = bf16[2,8,40,128]{3,2,1,0:T(8,128)(2,1)S(1)} collective-permute-done((bf16[2,8,40,128]{3,2,1,0:T(8,128)(2,1)}, bf16[2,8,40,128]{3,2,1,0:T(8,128)(2,1)S(1)}, u32[]{:S(2)}, u32[]{:S(2)}) %collective-permute-start.5) | collective-permute-done | bytes 163872 | tf_op jit(solution)/shard_map/ppermute | solution.py:62
  96.5 2.2 fusion.7
  99.5 3.6 %collective-permute-start.3 = (bf16[80,896]{1,0:T(8,128)(2,1)S(1)}, bf16[80,896]{1,0:T(8,128)(2,1)S(1)}, u32[]{:S(2)}, u32[]{:S(2)}) collective-permute-start(bf16[80,896]{1,0:T(8,128)(2,1)S(1)} %slice.138), channel_id=1, source_target_pairs={{0,2},{2,0},{1,3},{3,1},{4,6},{6,4},{5,7},{7,5},{8,10},{10,8},{9,1... | collective-permute-start | bytes 430088 | tf_op jit(solution)/shard_map/ppermute | solution.py:62
  103.1 1.1 fusion.9
  104.2 2.2 collective-permute-start.7
  106.8 39.8 %all_gather.3 = bf16[320,896]{1,0:T(8,128)(2,1)S(1)} all-gather(bf16[40,896]{1,0:T(8,128)(2,1)S(1)} %fusion.35), channel_id=1, replica_groups=mesh['ep'=16,'za'=8,'zb'=2,'core'=2] {'za'}, dimensions={0}, use_global_device_ids=true | all-gather | bytes 645120 | tf_op jit(solution)/shard_map/all_gather | solution.py:163
  148.1 1.1 pad_maximum_fusion
  149.1 7.9 %all-to-all-start.2 = ((bf16[64,56,128]{2,1,0:T(8,128)(2,1)}), bf16[64,56,128]{2,1,0:T(8,128)(2,1)S(1)}, u32[]{:S(2)}, u32[]{:S(2)}) async-start(bf16[64,56,128]{2,1,0:T(8,128)(2,1)} %bitcast.24), calls=%async_computation.2 | async-start | bytes 1835008 | tf_op jit(solution)/shard_map/all_to_all | solution.py:166
  157.1 1.5 convolution_add_fusion.2
  159.1 2.0 collective-permute-start.8
  161.1 2.7 %shard_map.102 = (bf16[160,2048]{1,0:T(8,128)(2,1)}, bf16[160,2048]{1,0:T(8,128)(2,1)}) custom-call(s32[1]{0:T(128)} %bitcast.own_ref, bf16[160,4096]{1,0:T(8,128)(2,1)} %weight.1), custom_call_target="tpu_custom_call" | custom-call | tf_op jit(solution)/shard_map/pallas_call | solution.py:52
  163.8 2.4 collective-permute-start.9
  166.8 1.4 collective-permute-done.9
  168.6 1.1 copy.40
  171.1 66.4 %reduce-scatter.2.cloned.1.call-done = bf16[1,224,128]{2,1,0:T(8,128)(2,1)} async-done(((bf16[16,224,128]{2,1,0:T(8,128)(2,1)}), bf16[1,224,128]{2,1,0:T(8,128)(2,1)}) %reduce-scatter.2.cloned.1.call-update) | async-done | bytes 57360 | tf_op jit(solution)/shard_map/reduce_scatter | solution.py:152
  237.5 2.0 fusion.6
  (59 shorter events, 6.2 us)
Async XLA Ops:
  8.2 40.1 %all-to-all-start = ((bf16[8,224,128]{2,1,0:T(8,128)(2,1)}), bf16[8,224,128]{2,1,0:T(8,128)(2,1)S(1)}, u32[]{:S(2)}, u32[]{:S(2)}) async-start(bf16[8,224,128]{2,1,0:T(8,128)(2,1)} %broadcast_in_dim.21), calls=%async_computation | async-start | bytes 917504 | tf_op jit(solution)/shard_map/all_to_all | solution.py:93
  50.3 33.1 %all-to-all-start.1 = ((bf16[16,56,1024]{2,1,0:T(8,128)(2,1)}), bf16[16,56,1024]{2,1,0:T(8,128)(2,1)S(1)}, u32[]{:S(2)}, u32[]{:S(2)}) async-start(bf16[16,56,1024]{2,1,0:T(8,128)(2,1)} %bitcast.115), calls=%async_computation.1 | async-start | bytes 3670016 | tf_op jit(solution)/shard_map/all_to_all | solution.py:135
  60.1 8.4 %copy-start.8 = (bf16[2,8,40,128]{3,2,1,0:T(8,128)(2,1)S(1)}, bf16[2,8,40,128]{3,2,1,0:T(8,128)(2,1)}, u32[]{:S(2)}) copy-start(bf16[2,8,40,128]{3,2,1,0:T(8,128)(2,1)} %get-tuple-element.21) | copy-start | bytes 491524
  60.1 10.3 %copy-start.2 = (bf16[2,40,1024]{2,1,0:T(8,128)(2,1)S(1)}, bf16[2,40,1024]{2,1,0:T(8,128)(2,1)}, u32[]{:S(2)}) copy-start(bf16[2,40,1024]{2,1,0:T(8,128)(2,1)} %get-tuple-element.18) | copy-start | bytes 491524
  60.1 10.3 %collective-permute-start = (bf16[2,2,40,1024]{3,2,1,0:T(8,128)(2,1)}, bf16[2,2,40,1024]{3,2,1,0:T(8,128)(2,1)S(1)}, u32[]{:S(2)}, u32[]{:S(2)}) collective-permute-start(bf16[2,2,40,1024]{3,2,1,0:T(8,128)(2,1)} %get-tuple-element.19), channel_id=1, source_target_pairs={{0,1},{1,0},{2,3},{3,2},{4,5},{5,4},{6,7},{7,6},{8,9},{9,8},{10,11... | collective-permute-start | bytes 983048 | tf_op jit(solution)/shard_map/ppermute | solution.py:62
  66.1 30.4 %collective-permute-start.6 = (bf16[2,320,1024]{2,1,0:T(8,128)(2,1)}, bf16[2,320,1024]{2,1,0:T(8,128)(2,1)}, u32[]{:S(2)}, u32[]{:S(2)}) collective-permute-start(bf16[2,320,1024]{2,1,0:T(8,128)(2,1)} %get-tuple-element.24), channel_id=1, source_target_pairs={{0,1},{1,0},{2,3},{3,2},{4,5},{5,4},{6,7},{7,6},{8,9},{9,8},{10,11... | collective-permute-start | bytes 3932168 | tf_op jit(solution)/shard_map/ppermute | solution.py:62
  68.5 6.5 %collective-permute-start.4 = (bf16[2,8,40,128]{3,2,1,0:T(8,128)(2,1)S(1)}, bf16[2,8,40,128]{3,2,1,0:T(8,128)(2,1)S(1)}, u32[]{:S(2)}, u32[]{:S(2)}) collective-permute-start(bf16[2,8,40,128]{3,2,1,0:T(8,128)(2,1)S(1)} %copy-done.8), channel_id=1, source_target_pairs={{0,1},{1,0},{2,3},{3,2},{4,5},{5,4},{6,7},{7,6},{8,9},{9,8},{10,11... | collective-permute-start | bytes 491528 | tf_op jit(solution)/shard_map/ppermute | solution.py:62
  70.5 12.9 %collective-permute-start.1 = (bf16[2,2,40,1024]{3,2,1,0:T(8,128)(2,1)S(1)}, bf16[2,2,40,1024]{3,2,1,0:T(8,128)(2,1)S(1)}, u32[]{:S(2)}, u32[]{:S(2)}) collective-permute-start(bf16[2,2,40,1024]{3,2,1,0:T(8,128)(2,1)S(1)} %pad_maximum_fusion.2), channel_id=1, source_target_pairs={{0,2},{2,0},{1,3},{3,1},{4,6},{6,4},{5,7},{7,5},{8,10},{10,8},{9,1... | collective-permute-start | bytes 983048 | tf_op jit(solution)/shard_map/ppermute | solution.py:62
  75.1 12.0 %copy-start.4 = (bf16[8,40,128]{2,1,0:T(8,128)(2,1)S(1)}, bf16[8,40,128]{2,1,0:T(8,128)(2,1)}, u32[]{:S(2)}) copy-start(bf16[8,40,128]{2,1,0:T(8,128)(2,1)} %get-tuple-element.22) | copy-start | bytes 245764
  83.4 13.0 %copy-start.3 = (bf16[8,40,128]{2,1,0:T(8,128)(2,1)S(1)}, bf16[8,40,128]{2,1,0:T(8,128)(2,1)}, u32[]{:S(2)}) copy-start(bf16[8,40,128]{2,1,0:T(8,128)(2,1)} %get-tuple-element.20) | copy-start | bytes 245764
  85.0 13.7 %copy-start.1 = (bf16[2,40,1024]{2,1,0:T(8,128)(2,1)S(1)}, bf16[2,40,1024]{2,1,0:T(8,128)(2,1)}, u32[]{:S(2)}) copy-start(bf16[2,40,1024]{2,1,0:T(8,128)(2,1)} %get-tuple-element.17) | copy-start | bytes 491524
  85.0 13.7 %collective-permute-start.2 = (f32[160,896]{1,0:T(8,128)}, f32[160,896]{1,0:T(8,128)S(1)}, u32[]{:S(2)}, u32[]{:S(2)}) collective-permute-start(f32[160,896]{1,0:T(8,128)} %fusion.29), channel_id=1, source_target_pairs={{0,1},{1,0},{2,3},{3,2},{4,5},{5,4},{6,7},{7,6},{8,9},{9,8},{10,11... | collective-permute-start | bytes 1720328 | tf_op jit(solution)/shard_map/ppermute | solution.py:62
  87.7 8.7 %collective-permute-start.5 = (bf16[2,8,40,128]{3,2,1,0:T(8,128)(2,1)}, bf16[2,8,40,128]{3,2,1,0:T(8,128)(2,1)S(1)}, u32[]{:S(2)}, u32[]{:S(2)}) collective-permute-start(bf16[2,8,40,128]{3,2,1,0:T(8,128)(2,1)} %pad_maximum_fusion.4), channel_id=1, source_target_pairs={{0,2},{2,0},{1,3},{3,1},{4,6},{6,4},{5,7},{7,5},{8,10},{10,8},{9,1... | collective-permute-start | bytes 491528 | tf_op jit(solution)/shard_map/ppermute | solution.py:62
  98.7 4.5 %copy-start.6 = (bf16[2,320,1024]{2,1,0:T(8,128)(2,1)S(1)}, bf16[2,320,1024]{2,1,0:T(8,128)(2,1)}, u32[]{:S(2)}) copy-start(bf16[2,320,1024]{2,1,0:T(8,128)(2,1)} %get-tuple-element.23) | copy-start | bytes 3932164
  99.5 7.2 %collective-permute-start.3 = (bf16[80,896]{1,0:T(8,128)(2,1)S(1)}, bf16[80,896]{1,0:T(8,128)(2,1)S(1)}, u32[]{:S(2)}, u32[]{:S(2)}) collective-permute-start(bf16[80,896]{1,0:T(8,128)(2,1)S(1)} %slice.138), channel_id=1, source_target_pairs={{0,2},{2,0},{1,3},{3,1},{4,6},{6,4},{5,7},{7,5},{8,10},{10,8},{9,1... | collective-permute-start | bytes 430088 | tf_op jit(solution)/shard_map/ppermute | solution.py:62
  104.2 52.9 %collective-permute-start.7 = (bf16[8,224,128]{2,1,0:T(8,128)(2,1)S(1)}, bf16[8,224,128]{2,1,0:T(8,128)(2,1)S(1)}, u32[]{:S(2)}, u32[]{:S(2)}) collective-permute-start(bf16[8,224,128]{2,1,0:T(8,128)(2,1)S(1)} %all-to-all-done), channel_id=1, source_target_pairs={{0,2},{2,0},{1,3},{3,1},{4,6},{6,4},{5,7},{7,5},{8,10},{10,8},{9,1... | collective-permute-start | bytes 1376264 | tf_op jit(solution)/shard_map/ppermute | solution.py:62
  148.1 9.0 %copy-start.10 = (f32[320,224]{1,0:T(8,128)S(1)}, f32[320,224]{1,0:T(8,128)}, u32[]{:S(2)}) copy-start(f32[320,224]{1,0:T(8,128)} %fusion.7) | copy-start | bytes 860164
  149.1 9.5 %copy-start.7 = (bf16[2,320,1024]{2,1,0:T(8,128)(2,1)S(1)}, bf16[2,320,1024]{2,1,0:T(8,128)(2,1)}, u32[]{:S(2)}) copy-start(bf16[2,320,1024]{2,1,0:T(8,128)(2,1)} %get-tuple-element.23) | copy-start | bytes 3932164
  149.1 88.3 %all-to-all-start.2 = ((bf16[64,56,128]{2,1,0:T(8,128)(2,1)}), bf16[64,56,128]{2,1,0:T(8,128)(2,1)S(1)}, u32[]{:S(2)}, u32[]{:S(2)}) async-start(bf16[64,56,128]{2,1,0:T(8,128)(2,1)} %bitcast.24), calls=%async_computation.2 | async-start | bytes 1835008 | tf_op jit(solution)/shard_map/all_to_all | solution.py:166
  157.1 80.4 %reduce-scatter.2.cloned.1.call-start = ((), (), s32[]{:S(2)}) async-start(), calls=%async_computation.4 | async-start | bytes 974848 | tf_op jit(solution)/shard_map/reduce_scatter | solution.py:152
  157.1 1.5 copy-start.11
  159.1 7.2 %collective-permute-start.8 = (f32[2,320,224]{2,1,0:T(8,128)S(1)}, f32[2,320,224]{2,1,0:T(8,128)S(1)}, u32[]{:S(2)}, u32[]{:S(2)}) collective-permute-start(f32[2,320,224]{2,1,0:T(8,128)S(1)} %pad_maximum_fusion.1), channel_id=1, source_target_pairs={{0,1},{1,0},{2,3},{3,2},{4,5},{5,4},{6,7},{7,6},{8,9},{9,8},{10,11... | collective-permute-start | bytes 1720328 | tf_op jit(solution)/shard_map/ppermute | solution.py:62
  163.8 2.5 %copy-start = (bf16[160,2048]{1,0:T(8,128)(2,1)S(1)}, bf16[160,2048]{1,0:T(8,128)(2,1)}, u32[]{:S(2)}) copy-start(bf16[160,2048]{1,0:T(8,128)(2,1)} %get-tuple-element.27) | copy-start | bytes 1966084
  163.8 4.3 %collective-permute-start.9 = (bf16[160,2048]{1,0:T(8,128)(2,1)}, bf16[160,2048]{1,0:T(8,128)(2,1)S(1)}, u32[]{:S(2)}, u32[]{:S(2)}) collective-permute-start(bf16[160,2048]{1,0:T(8,128)(2,1)} %get-tuple-element.28), channel_id=1, source_target_pairs={{0,1},{1,0},{2,3},{3,2},{4,5},{5,4},{6,7},{7,6},{8,9},{9,8},{10,11... | collective-permute-start | bytes 1966088 | tf_op jit(solution)/shard_map/ppermute | solution.py:62
  168.6 1.1 copy-start.5
  170.4 0.7 copy-start.9
Sparse Core Ops, SparseCore 0:
  169.9 67.5 reduce-scatter.1

commit v2 on v1

--- a/solution.py
+++ b/solution.py
@@ -14,18 +14,21 @@
 LANES = 128
 
 
-def expert_kernel(own_ref, gate, up, down, gu_own, gu_far, gu_near, own_out, far_out, near_out):
+def expert_kernel(own_ref, gate, up, down, gu_own, turn_own, far, near):
     own = own_ref[0]
-    pairs = (gu_own, gu_near.at[0], gu_far, gu_near.at[1])
-    turns = (own_out, near_out.at[0], far_out, near_out.at[1])
-    for k in range(4):
-        for j in range(own_out.shape[0]):
+    packs = (None, near.at[0], far, near.at[1])
+    for k, pack in enumerate(packs):
+        for j in range(turn_own.shape[0]):
             tile = j * 4 + (own ^ k)
             start = pl.multiple_of(tile * LANES, LANES)
             at = slice(j * LANES, (j + 1) * LANES)
-            pairs[k][0, :, at] = gate[:, pl.ds(start, LANES)]
-            pairs[k][1, :, at] = up[:, pl.ds(start, LANES)]
-            turns[k][j] = down[tile]
+            pair = pack if k else gu_own
+            pair[0, :, at] = gate[:, pl.ds(start, LANES)]
+            pair[1, :, at] = up[:, pl.ds(start, LANES)]
+            if k:
+                pack[2, :, at] = down[tile]
+            else:
+                turn_own[j] = down[tile]
 
 
 def dense_kernel(own_ref, gate, up, keep, give):
@@ -96,24 +99,25 @@
     mine = flat(tiles)
 
     down = down_weight[0].reshape(n_za * 4, hid, width)
-    pair, turn = (2, hid, part), (n_za, hid, width)
-    gu_own, gu_far, gu_near, turn_own, turn_far, turn_near = split_up(
+    pack = (3, hid, part)
+    gu_own, turn_own, far, near = split_up(
         expert_kernel,
         quad,
-        [pair, pair, (2, *pair), turn, turn, (2, *turn)],
+        [(2, hid, part), (n_za, hid, width), pack, (2, *pack)],
         gate_weight[0],
         up_weight[0],
         down,
     )
-    gu_near = swap(gu_near, "core", 2, 1)
-    relay = jnp.stack([gu_far, gu_near[1]])
-    gu_far = swap(relay, "zb", 2, 1)
-    gu = [gu_own, gu_near[0], gu_far[0], gu_far[1]]
+    near = swap(near, "core", 2, 1)
+    far = jnp.stack([far, near[1]])
+    far = swap(far, "zb", 2, 1)
+    gu = [gu_own, near[0, :2], far[0, :2], far[1, :2]]
     gu = [x.reshape(2 * hid, part) for x in gu]
-    turn_near = swap(turn_near, "core", 2, 1)
-    turn_far = swap(jnp.stack([turn_far, turn_near[1]]), "zb", 2, 1)
-    turned = jnp.stack([turn_own, turn_near[0], turn_far[0], turn_far[1]])
-    turned = turned.reshape(4, n_za * hid, width)
+    turned = [
+        jnp.moveaxis(x.reshape(hid, n_za, width), 1, 0)
+        for x in (near[0, 2], far[0, 2], far[1, 2])
+    ]
+    turned = jnp.stack([turn_own, *turned]).reshape(4, n_za * hid, width)
     columns = [
         lax.dynamic_index_in_dim(turned, quad ^ q, 0, keepdims=False) for q in range(4)
     ]
@@ -167,8 +171,9 @@
 
     token = lax.broadcasted_iota(jnp.int32, (rows, experts * slots), 0)
     spread = jnp.where(token == chosen[None, :], pick_weights.reshape(1, -1), 0.0)
-    spread = jnp.tile(spread.astype(jnp.bfloat16), (1, 4))
-    mixture = dot(spread, back.reshape(4 * experts * slots, width), PLAIN)
+    parts = back.reshape(4, experts * slots, width).astype(jnp.float32)
+    results = jnp.sum(parts, axis=0).astype(jnp.bfloat16)
+    mixture = dot(spread.astype(jnp.bfloat16), results, PLAIN)
     mixed = mixture + jax.nn.sigmoid(branch_gate)[None, :] * dense_out.astype(jnp.float32)
     return mixed.astype(jnp.bfloat16)
 

time: 247 us -> 237 us (0.960)
  starting transfers between devices: 57.3 us -> 50.6 us
  waiting for transfers between devices: 106 us -> 101 us
    ppermute x10 -> x8, starting transfers between devices: 26.8 us -> 20.6 us  [swap(): return lax.ppermute(x, axes, [(i, i ^ k) for i in range(size)])]
    ppermute x10 -> x8, waiting for transfers between devices: 15 us -> 9.3 us  [swap(): return lax.ppermute(x, axes, [(i, i ^ k) for i in range(size)])]
  transfers between devices with their start and end apart: 14 -> 12, of which waited for: 6 -> 7; matrix products, arithmetic and copies ran while one was open for 6% -> 7% of each run, Pallas kernels for 4% -> 4%
where the time goes in v2:
time: 237 us; the launch traced here: 236 us
  waiting for transfers between devices  101 us (43%)
  starting transfers between devices  50.6 us (21%)
  blocking collectives  40 us (17%)
  between operations  13.8 us (6%)
  matrix products  13.7 us (6%)
  Pallas kernels  9.08 us (4%)
  local copies, waits for them, and re-layouts  4.78 us (2%)
  other arithmetic  3.42 us (1%)
    reduce_scatter x1, waiting for transfers between devices, per_device(): lax.psum_scatter(jnp.moveaxis(wide, 1, 0), ('za', 'zb'), scatter_dimensio...  65.8 us
    all_gather x1, blocking collectives, per_device(): units = lax.all_gather(hidden, 'za', axis=0, tiled=True)  40 us
    all_to_all x1, waiting for transfers between devices, per_device(): lax.all_to_all(jnp.broadcast_to(tokens, (n_za, rows, width)), 'za', split...  24.3 us
    ppermute x8, starting transfers between devices, swap(): return lax.ppermute(x, axes, [(i, i ^ k) for i in range(size)])  20.6 us
    all_to_all x1, starting transfers between devices, per_device(): lax.all_to_all(jnp.broadcast_to(tokens, (n_za, rows, width)), 'za', split...  15.1 us
    dot_general x14, matrix products, dot(): return lax.dot_general(a, b, dims, preferred_element_type=jnp.float32)  13.7 us
    ppermute x8, waiting for transfers between devices, swap(): return lax.ppermute(x, axes, [(i, i ^ k) for i in range(size)])  9.3 us
    pallas_call x3, Pallas kernels, split_up(): pl.pallas_call(kernel, out_shape=[jax.ShapeDtypeStruct(shape, jnp.bfloat1...  9.08 us
  transfers between devices with their start and end apart: 12, of which 7 were waited for; matrix products, arithmetic and copies ran while one was open for 7% of the time, Pallas kernels for 4%

profile of v2, /device:TPU:2, one launch (start us, length us, event | category | flops | bytes accessed | tf_op | source)
XLA Modules:
  0.0 236.4 jit_solution(1419259047225490055)
XLA Ops:
  6.5 1.7 broadcast_in_dim.21
  8.2 15.1 %all-to-all-start = ((bf16[8,224,128]{2,1,0:T(8,128)(2,1)}), bf16[8,224,128]{2,1,0:T(8,128)(2,1)S(1)}, u32[]{:S(2)}, u32[]{:S(2)}) async-start(bf16[8,224,128]{2,1,0:T(8,128)(2,1)} %broadcast_in_dim.21), calls=%async_computation | async-start | bytes 917504 | tf_op jit(solution)/shard_map/all_to_all | solution.py:96
  24.1 24.3 %all-to-all-done = bf16[8,224,128]{2,1,0:T(8,128)(2,1)S(1)} async-done(((bf16[8,224,128]{2,1,0:T(8,128)(2,1)}), bf16[8,224,128]{2,1,0:T(8,128)(2,1)S(1)}, u32[]{:S(2)}, u32[]{:S(2)}) %all-to-all-start) | async-done | bytes 458784 | tf_op jit(solution)/shard_map/all_to_all | solution.py:96
  48.3 1.9 convolution_convert_fusion
  50.3 7.5 %all-to-all-start.1 = ((bf16[16,56,1024]{2,1,0:T(8,128)(2,1)}), bf16[16,56,1024]{2,1,0:T(8,128)(2,1)S(1)}, u32[]{:S(2)}, u32[]{:S(2)}) async-start(bf16[16,56,1024]{2,1,0:T(8,128)(2,1)} %bitcast.135), calls=%async_computation.1 | async-start | bytes 3670016 | tf_op jit(solution)/shard_map/all_to_all | solution.py:139
  57.8 2.3 shard_map.100
  60.1 1.9 collective-permute-start
  62.0 2.0 collective-permute-done
  64.1 2.0 pad_maximum_fusion.2
  66.1 4.5 %collective-permute-start.1 = (bf16[2,3,40,1024]{3,2,1,0:T(8,128)(2,1)}, bf16[2,3,40,1024]{3,2,1,0:T(8,128)(2,1)S(1)}, u32[]{:S(2)}, u32[]{:S(2)}) collective-permute-start(bf16[2,3,40,1024]{3,2,1,0:T(8,128)(2,1)} %pad_maximum_fusion.2), channel_id=1, source_target_pairs={{0,2},{2,0},{1,3},{3,1},{4,6},{6,4},{5,7},{7,5},{8,10},{10,8},{9,1... | collective-permute-start | bytes 1474568 | tf_op jit(solution)/shard_map/ppermute | solution.py:65
  70.6 4.0 %shard_map.101 = (bf16[2,320,1024]{2,1,0:T(8,128)(2,1)}, bf16[2,320,1024]{2,1,0:T(8,128)(2,1)}) custom-call(s32[1]{0:T(128)} %bitcast.own_ref, bf16[160,4096]{1,0:T(8,128)(2,1)} %gate.1, bf16[160,4096]{1,0:T(8,128)(2,1)} %up.1), custom_call_target="tpu_custom_call" | custom-call | tf_op jit(solution)/shard_map/pallas_call | solution.py:55
  74.5 1.9 collective-permute-start.4
  77.5 4.8 %collective-permute-done.1 = bf16[2,3,40,1024]{3,2,1,0:T(8,128)(2,1)S(1)} collective-permute-done((bf16[2,3,40,1024]{3,2,1,0:T(8,128)(2,1)}, bf16[2,3,40,1024]{3,2,1,0:T(8,128)(2,1)S(1)}, u32[]{:S(2)}, u32[]{:S(2)}) %collective-permute-start.1) | collective-permute-done | bytes 491552 | tf_op jit(solution)/shard_map/ppermute | solution.py:65
  83.1 2.1 collective-permute-start.2
  85.3 2.2 fusion.7
  88.3 3.6 %collective-permute-start.3 = (bf16[80,896]{1,0:T(8,128)(2,1)S(1)}, bf16[80,896]{1,0:T(8,128)(2,1)S(1)}, u32[]{:S(2)}, u32[]{:S(2)}) collective-permute-start(bf16[80,896]{1,0:T(8,128)(2,1)S(1)} %slice.143), channel_id=1, source_target_pairs={{0,2},{2,0},{1,3},{3,1},{4,6},{6,4},{5,7},{7,5},{8,10},{10,8},{9,1... | collective-permute-start | bytes 430088 | tf_op jit(solution)/shard_map/ppermute | solution.py:65
  92.0 1.1 fusion.9
  93.1 2.2 collective-permute-start.5
  95.3 1.1 collective-permute-done.3
  96.5 40.0 %all_gather.3 = bf16[320,896]{1,0:T(8,128)(2,1)S(1)} all-gather(bf16[40,896]{1,0:T(8,128)(2,1)S(1)} %fusion.38), channel_id=1, replica_groups=mesh['ep'=16,'za'=8,'zb'=2,'core'=2] {'za'}, dimensions={0}, use_global_device_ids=true | all-gather | bytes 645120 | tf_op jit(solution)/shard_map/all_gather | solution.py:167
  138.1 1.1 pad_maximum_fusion
  139.1 7.3 %all-to-all-start.2 = ((bf16[64,56,128]{2,1,0:T(8,128)(2,1)}), bf16[64,56,128]{2,1,0:T(8,128)(2,1)S(1)}, u32[]{:S(2)}, u32[]{:S(2)}) async-start(bf16[64,56,128]{2,1,0:T(8,128)(2,1)} %bitcast.27), calls=%async_computation.2 | async-start | bytes 1835008 | tf_op jit(solution)/shard_map/all_to_all | solution.py:170
  146.5 1.5 convolution_add_fusion.2
  148.0 1.3 convolution_add_fusion.3
  149.4 2.0 collective-permute-start.6
  151.4 2.8 %shard_map.102 = (bf16[160,2048]{1,0:T(8,128)(2,1)}, bf16[160,2048]{1,0:T(8,128)(2,1)}) custom-call(s32[1]{0:T(128)} %bitcast.own_ref, bf16[160,4096]{1,0:T(8,128)(2,1)} %weight.1), custom_call_target="tpu_custom_call" | custom-call | tf_op jit(solution)/shard_map/pallas_call | solution.py:55
  154.2 2.4 %collective-permute-start.7 = (bf16[160,2048]{1,0:T(8,128)(2,1)}, bf16[160,2048]{1,0:T(8,128)(2,1)S(1)}, u32[]{:S(2)}, u32[]{:S(2)}) collective-permute-start(bf16[160,2048]{1,0:T(8,128)(2,1)} %get-tuple-element.24), channel_id=1, source_target_pairs={{0,1},{1,0},{2,3},{3,2},{4,5},{5,4},{6,7},{7,6},{8,9},{9,8},{10,11... | collective-permute-start | bytes 1966088 | tf_op jit(solution)/shard_map/ppermute | solution.py:65
  157.2 1.4 collective-permute-done.7
  159.0 1.1 copy.48
  160.3 1.6 all-to-all-done.2
  162.0 65.8 %reduce-scatter.2.cloned.1.call-done = bf16[1,224,128]{2,1,0:T(8,128)(2,1)} async-done(((bf16[16,224,128]{2,1,0:T(8,128)(2,1)}), bf16[1,224,128]{2,1,0:T(8,128)(2,1)}) %reduce-scatter.2.cloned.1.call-update) | async-done | bytes 57360 | tf_op jit(solution)/shard_map/reduce_scatter | solution.py:156
  227.8 1.7 fusion.6
  (54 shorter events, 6.4 us)
Async XLA Ops:
  8.2 40.1 %all-to-all-start = ((bf16[8,224,128]{2,1,0:T(8,128)(2,1)}), bf16[8,224,128]{2,1,0:T(8,128)(2,1)S(1)}, u32[]{:S(2)}, u32[]{:S(2)}) async-start(bf16[8,224,128]{2,1,0:T(8,128)(2,1)} %broadcast_in_dim.21), calls=%async_computation | async-start | bytes 917504 | tf_op jit(solution)/shard_map/all_to_all | solution.py:96
  50.3 32.0 %all-to-all-start.1 = ((bf16[16,56,1024]{2,1,0:T(8,128)(2,1)}), bf16[16,56,1024]{2,1,0:T(8,128)(2,1)S(1)}, u32[]{:S(2)}, u32[]{:S(2)}) async-start(bf16[16,56,1024]{2,1,0:T(8,128)(2,1)} %bitcast.135), calls=%async_computation.1 | async-start | bytes 3670016 | tf_op jit(solution)/shard_map/all_to_all | solution.py:139
  60.1 4.0 %collective-permute-start = (bf16[2,3,40,1024]{3,2,1,0:T(8,128)(2,1)}, bf16[2,3,40,1024]{3,2,1,0:T(8,128)(2,1)S(1)}, u32[]{:S(2)}, u32[]{:S(2)}) collective-permute-start(bf16[2,3,40,1024]{3,2,1,0:T(8,128)(2,1)} %get-tuple-element.17), channel_id=1, source_target_pairs={{0,1},{1,0},{2,3},{3,2},{4,5},{5,4},{6,7},{7,6},{8,9},{9,8},{10,11... | collective-permute-start | bytes 1474568 | tf_op jit(solution)/shard_map/ppermute | solution.py:65
  64.1 12.4 %copy-start.1 = (bf16[2,3,40,1024]{3,2,1,0:T(8,128)(2,1)}, bf16[2,3,40,1024]{3,2,1,0:T(8,128)(2,1)S(1)}, u32[]{:S(2)}) copy-start(bf16[2,3,40,1024]{3,2,1,0:T(8,128)(2,1)S(1)} %collective-permute-done) | copy-start | bytes 1474564
  66.1 16.2 %collective-permute-start.1 = (bf16[2,3,40,1024]{3,2,1,0:T(8,128)(2,1)}, bf16[2,3,40,1024]{3,2,1,0:T(8,128)(2,1)S(1)}, u32[]{:S(2)}, u32[]{:S(2)}) collective-permute-start(bf16[2,3,40,1024]{3,2,1,0:T(8,128)(2,1)} %pad_maximum_fusion.2), channel_id=1, source_target_pairs={{0,2},{2,0},{1,3},{3,1},{4,6},{6,4},{5,7},{7,5},{8,10},{10,8},{9,1... | collective-permute-start | bytes 1474568 | tf_op jit(solution)/shard_map/ppermute | solution.py:65
  74.5 10.8 %collective-permute-start.4 = (bf16[2,320,1024]{2,1,0:T(8,128)(2,1)}, bf16[2,320,1024]{2,1,0:T(8,128)(2,1)}, u32[]{:S(2)}, u32[]{:S(2)}) collective-permute-start(bf16[2,320,1024]{2,1,0:T(8,128)(2,1)} %get-tuple-element.20), channel_id=1, source_target_pairs={{0,1},{1,0},{2,3},{3,2},{4,5},{5,4},{6,7},{7,6},{8,9},{9,8},{10,11... | collective-permute-start | bytes 3932168 | tf_op jit(solution)/shard_map/ppermute | solution.py:65
  82.3 2.9 %copy-start.3 = (bf16[8,40,128]{2,1,0:T(8,128)(2,1)S(1)}, bf16[8,40,128]{2,1,0:T(8,128)(2,1)}, u32[]{:S(2)}) copy-start(bf16[8,40,128]{2,1,0:T(8,128)(2,1)} %get-tuple-element.18) | copy-start | bytes 245764
  83.1 4.4 %copy-start.2 = (bf16[2,40,1024]{2,1,0:T(8,128)(2,1)S(1)}, bf16[2,40,1024]{2,1,0:T(8,128)(2,1)}, u32[]{:S(2)}) copy-start(bf16[2,40,1024]{2,1,0:T(8,128)(2,1)} %get-tuple-element.15) | copy-start | bytes 491524
  83.1 4.4 %collective-permute-start.2 = (f32[160,896]{1,0:T(8,128)S(1)}, f32[160,896]{1,0:T(8,128)S(1)}, u32[]{:S(2)}, u32[]{:S(2)}) collective-permute-start(f32[160,896]{1,0:T(8,128)S(1)} %fusion.32), channel_id=1, source_target_pairs={{0,1},{1,0},{2,3},{3,2},{4,5},{5,4},{6,7},{7,6},{8,9},{9,8},{10,11... | collective-permute-start | bytes 1720328 | tf_op jit(solution)/shard_map/ppermute | solution.py:65
  87.5 4.5 %copy-start.5 = (bf16[2,320,1024]{2,1,0:T(8,128)(2,1)S(1)}, bf16[2,320,1024]{2,1,0:T(8,128)(2,1)}, u32[]{:S(2)}) copy-start(bf16[2,320,1024]{2,1,0:T(8,128)(2,1)} %get-tuple-element.19) | copy-start | bytes 3932164
  88.3 8.1 %collective-permute-start.3 = (bf16[80,896]{1,0:T(8,128)(2,1)S(1)}, bf16[80,896]{1,0:T(8,128)(2,1)S(1)}, u32[]{:S(2)}, u32[]{:S(2)}) collective-permute-start(bf16[80,896]{1,0:T(8,128)(2,1)S(1)} %slice.143), channel_id=1, source_target_pairs={{0,2},{2,0},{1,3},{3,1},{4,6},{6,4},{5,7},{7,5},{8,10},{10,8},{9,1... | collective-permute-start | bytes 430088 | tf_op jit(solution)/shard_map/ppermute | solution.py:65
  93.1 53.4 %collective-permute-start.5 = (bf16[8,224,128]{2,1,0:T(8,128)(2,1)S(1)}, bf16[8,224,128]{2,1,0:T(8,128)(2,1)S(1)}, u32[]{:S(2)}, u32[]{:S(2)}) collective-permute-start(bf16[8,224,128]{2,1,0:T(8,128)(2,1)S(1)} %all-to-all-done), channel_id=1, source_target_pairs={{0,2},{2,0},{1,3},{3,1},{4,6},{6,4},{5,7},{7,5},{8,10},{10,8},{9,1... | collective-permute-start | bytes 1376264 | tf_op jit(solution)/shard_map/ppermute | solution.py:65
  138.1 8.5 %copy-start.8 = (f32[320,224]{1,0:T(8,128)S(1)}, f32[320,224]{1,0:T(8,128)}, u32[]{:S(2)}) copy-start(f32[320,224]{1,0:T(8,128)} %fusion.7) | copy-start | bytes 860164
  139.1 8.9 %copy-start.6 = (bf16[2,320,1024]{2,1,0:T(8,128)(2,1)S(1)}, bf16[2,320,1024]{2,1,0:T(8,128)(2,1)}, u32[]{:S(2)}) copy-start(bf16[2,320,1024]{2,1,0:T(8,128)(2,1)} %get-tuple-element.19) | copy-start | bytes 3932164
  139.1 22.8 %all-to-all-start.2 = ((bf16[64,56,128]{2,1,0:T(8,128)(2,1)}), bf16[64,56,128]{2,1,0:T(8,128)(2,1)S(1)}, u32[]{:S(2)}, u32[]{:S(2)}) async-start(bf16[64,56,128]{2,1,0:T(8,128)(2,1)} %bitcast.27), calls=%async_computation.2 | async-start | bytes 1835008 | tf_op jit(solution)/shard_map/all_to_all | solution.py:170
  146.5 81.3 %reduce-scatter.2.cloned.1.call-start = ((), (), s32[]{:S(2)}) async-start(), calls=%async_computation.4 | async-start | bytes 974848 | tf_op jit(solution)/shard_map/reduce_scatter | solution.py:156
  149.4 7.2 %collective-permute-start.6 = (f32[2,320,224]{2,1,0:T(8,128)S(1)}, f32[2,320,224]{2,1,0:T(8,128)S(1)}, u32[]{:S(2)}, u32[]{:S(2)}) collective-permute-start(f32[2,320,224]{2,1,0:T(8,128)S(1)} %pad_maximum_fusion.1), channel_id=1, source_target_pairs={{0,1},{1,0},{2,3},{3,2},{4,5},{5,4},{6,7},{7,6},{8,9},{9,8},{10,11... | collective-permute-start | bytes 1720328 | tf_op jit(solution)/shard_map/ppermute | solution.py:65
  154.2 2.5 %copy-start = (bf16[160,2048]{1,0:T(8,128)(2,1)S(1)}, bf16[160,2048]{1,0:T(8,128)(2,1)}, u32[]{:S(2)}) copy-start(bf16[160,2048]{1,0:T(8,128)(2,1)} %get-tuple-element.23) | copy-start | bytes 1966084
  154.2 4.3 %collective-permute-start.7 = (bf16[160,2048]{1,0:T(8,128)(2,1)}, bf16[160,2048]{1,0:T(8,128)(2,1)S(1)}, u32[]{:S(2)}, u32[]{:S(2)}) collective-permute-start(bf16[160,2048]{1,0:T(8,128)(2,1)} %get-tuple-element.24), channel_id=1, source_target_pairs={{0,1},{1,0},{2,3},{3,2},{4,5},{5,4},{6,7},{7,6},{8,9},{9,8},{10,11... | collective-permute-start | bytes 1966088 | tf_op jit(solution)/shard_map/ppermute | solution.py:65
  159.0 1.2 copy-start.4
  159.0 1.3 copy-start.7
Sparse Core Ops, SparseCore 0:
  160.3 67.4 reduce-scatter.1

commit v3 on v1

--- a/solution.py
+++ b/solution.py
@@ -114,16 +114,17 @@
     turn_far = swap(jnp.stack([turn_far, turn_near[1]]), "zb", 2, 1)
     turned = jnp.stack([turn_own, turn_near[0], turn_far[0], turn_far[1]])
     turned = turned.reshape(4, n_za * hid, width)
-    columns = [
-        lax.dynamic_index_in_dim(turned, quad ^ q, 0, keepdims=False) for q in range(4)
-    ]
+    columns = jnp.stack(
+        [lax.dynamic_index_in_dim(turned, quad ^ q, 0, keepdims=False) for q in range(4)]
+    )
     dense_keep, dense_give = split_up(
         dense_kernel, quad, [(2, 2 * dense_hid, part)] * 2, dense_gate, dense_up
     )
+    dense_came = swap(dense_give, "core", 2, 1)
+
     down_keep, down_give = split_up(
         down_kernel, quad, [(dense_hid, 2 * part)] * 2, dense_down
     )
-    dense_came = swap(dense_give, "core", 2, 1)
     down_came = swap(down_give, "core", 2, 1)
 
     chosen = picks.reshape(-1)
@@ -161,14 +162,16 @@
     hidden = (jax.nn.silu(gate_up[:hid]) * gate_up[hid:]).astype(jnp.bfloat16)
 
     units = lax.all_gather(hidden, "za", axis=0, tiled=True)
-    outgoing = jnp.stack([dot(units, c, FIRST).astype(jnp.bfloat16) for c in columns])
+    outgoing = jnp.einsum("kt,qkf->qtf", units, columns, preferred_element_type=jnp.float32)
+    outgoing = outgoing.astype(jnp.bfloat16)
     outgoing = outgoing.reshape(4 * experts, slots, width)
     back = lax.all_to_all(outgoing, ("zb", "core", "ep"), split_axis=0, concat_axis=0, tiled=True)
 
     token = lax.broadcasted_iota(jnp.int32, (rows, experts * slots), 0)
     spread = jnp.where(token == chosen[None, :], pick_weights.reshape(1, -1), 0.0)
-    spread = jnp.tile(spread.astype(jnp.bfloat16), (1, 4))
-    mixture = dot(spread, back.reshape(4 * experts * slots, width), PLAIN)
+    parts = back.reshape(4, experts * slots, width).astype(jnp.float32)
+    results = jnp.sum(parts, axis=0).astype(jnp.bfloat16)
+    mixture = dot(spread.astype(jnp.bfloat16), results, PLAIN)
     mixed = mixture + jax.nn.sigmoid(branch_gate)[None, :] * dense_out.astype(jnp.float32)
     return mixed.astype(jnp.bfloat16)
 

time: 247 us -> 239 us (0.968)
  waiting for transfers between devices: 106 us -> 100 us
    ppermute x10, waiting for transfers between devices: 15 us -> 8.65 us  [swap(): return lax.ppermute(x, axes, [(i, i ^ k) for i in range(size)])]
    dot_general x14 -> x10, matrix products: 13.8 us -> 13 us  [dot(): return lax.dot_general(a, b, dims, preferred_element_type=jnp.float32)]
where the time goes in v3:
time: 239 us; the launch traced here: 238 us
  waiting for transfers between devices  100 us (42%)
  starting transfers between devices  55.5 us (23%)
  blocking collectives  39.4 us (16%)
  between operations  13.8 us (6%)
  matrix products  13.7 us (6%)
  Pallas kernels  9.01 us (4%)
  local copies, waits for them, and re-layouts  5.08 us (2%)
    reduce_scatter x1, waiting for transfers between devices, per_device(): lax.psum_scatter(jnp.moveaxis(wide, 1, 0), ('za', 'zb'), scatter_dimensio...  65.4 us
    all_gather x1, blocking collectives, per_device(): units = lax.all_gather(hidden, 'za', axis=0, tiled=True)  39.4 us
    ppermute x10, starting transfers between devices, swap(): return lax.ppermute(x, axes, [(i, i ^ k) for i in range(size)])  25.1 us
    all_to_all x1, waiting for transfers between devices, per_device(): lax.all_to_all(jnp.broadcast_to(tokens, (n_za, rows, width)), 'za', split...  24.3 us
    all_to_all x1, starting transfers between devices, per_device(): lax.all_to_all(jnp.broadcast_to(tokens, (n_za, rows, width)), 'za', split...  15.1 us
    dot_general x10, matrix products, dot(): return lax.dot_general(a, b, dims, preferred_element_type=jnp.float32)  13 us
    pallas_call x3, Pallas kernels, split_up(): pl.pallas_call(kernel, out_shape=[jax.ShapeDtypeStruct(shape, jnp.bfloat1...  9.01 us
    ppermute x10, waiting for transfers between devices, swap(): return lax.ppermute(x, axes, [(i, i ^ k) for i in range(size)])  8.65 us
  transfers between devices with their start and end apart: 14, of which 6 were waited for; matrix products, arithmetic and copies ran while one was open for 6% of the time, Pallas kernels for 4%

profile of v3, /device:TPU:2, one launch (start us, length us, event | category | flops | bytes accessed | tf_op | source)
XLA Modules:
  0.0 237.5 jit_solution(15047417871672823517)
XLA Ops:
  6.5 1.6 broadcast_in_dim.21
  8.2 15.1 %all-to-all-start = ((bf16[8,224,128]{2,1,0:T(8,128)(2,1)}), bf16[8,224,128]{2,1,0:T(8,128)(2,1)S(1)}, u32[]{:S(2)}, u32[]{:S(2)}) async-start(bf16[8,224,128]{2,1,0:T(8,128)(2,1)} %broadcast_in_dim.21), calls=%async_computation | async-start | bytes 917504 | tf_op jit(solution)/shard_map/all_to_all | solution.py:93
  24.1 24.3 %all-to-all-done = bf16[8,224,128]{2,1,0:T(8,128)(2,1)S(1)} async-done(((bf16[8,224,128]{2,1,0:T(8,128)(2,1)}), bf16[8,224,128]{2,1,0:T(8,128)(2,1)S(1)}, u32[]{:S(2)}, u32[]{:S(2)}) %all-to-all-start) | async-done | bytes 458784 | tf_op jit(solution)/shard_map/all_to_all | solution.py:93
  48.3 1.9 convolution_convert_fusion
  50.3 7.5 %all-to-all-start.1 = ((bf16[16,56,1024]{2,1,0:T(8,128)(2,1)}), bf16[16,56,1024]{2,1,0:T(8,128)(2,1)S(1)}, u32[]{:S(2)}, u32[]{:S(2)}) async-start(bf16[16,56,1024]{2,1,0:T(8,128)(2,1)} %bitcast.95), calls=%async_computation.1 | async-start | bytes 3670016 | tf_op jit(solution)/shard_map/all_to_all | solution.py:136
  57.8 2.3 shard_map.100
  60.1 2.1 collective-permute-start.2
  62.2 3.9 %shard_map.101 = (bf16[2,320,1024]{2,1,0:T(8,128)(2,1)}, bf16[2,320,1024]{2,1,0:T(8,128)(2,1)}) custom-call(s32[1]{0:T(128)} %bitcast.own_ref, bf16[160,4096]{1,0:T(8,128)(2,1)} %gate.1, bf16[160,4096]{1,0:T(8,128)(2,1)} %up.1), custom_call_target="tpu_custom_call" | custom-call | tf_op jit(solution)/shard_map/pallas_call | solution.py:52
  66.1 2.4 %collective-permute-start.6 = (bf16[2,320,1024]{2,1,0:T(8,128)(2,1)}, bf16[2,320,1024]{2,1,0:T(8,128)(2,1)}, u32[]{:S(2)}, u32[]{:S(2)}) collective-permute-start(bf16[2,320,1024]{2,1,0:T(8,128)(2,1)} %get-tuple-element.24), channel_id=1, source_target_pairs={{0,1},{1,0},{2,3},{3,2},{4,5},{5,4},{6,7},{7,6},{8,9},{9,8},{10,11... | collective-permute-start | bytes 3932168 | tf_op jit(solution)/shard_map/ppermute | solution.py:62
  68.5 1.9 collective-permute-start
  70.5 4.5 %collective-permute-start.3 = (bf16[2,2,40,1024]{3,2,1,0:T(8,128)(2,1)S(1)}, bf16[2,2,40,1024]{3,2,1,0:T(8,128)(2,1)S(1)}, u32[]{:S(2)}, u32[]{:S(2)}) collective-permute-start(bf16[2,2,40,1024]{3,2,1,0:T(8,128)(2,1)S(1)} %pad_maximum_fusion.2), channel_id=1, source_target_pairs={{0,2},{2,0},{1,3},{3,1},{4,6},{6,4},{5,7},{7,5},{8,10},{10,8},{9,1... | collective-permute-start | bytes 983048 | tf_op jit(solution)/shard_map/ppermute | solution.py:62
  75.8 1.9 collective-permute-start.1
  77.7 5.9 %collective-permute-done.3 = bf16[2,2,40,1024]{3,2,1,0:T(8,128)(2,1)S(1)} collective-permute-done((bf16[2,2,40,1024]{3,2,1,0:T(8,128)(2,1)S(1)}, bf16[2,2,40,1024]{3,2,1,0:T(8,128)(2,1)S(1)}, u32[]{:S(2)}, u32[]{:S(2)}) %collective-permute-start.3) | collective-permute-done | bytes 327712 | tf_op jit(solution)/shard_map/ppermute | solution.py:62
  83.6 1.6 fusion.37
  85.2 2.0 collective-permute-start.4
  87.4 2.2 fusion.4
  90.4 3.9 %collective-permute-start.5 = (bf16[80,896]{1,0:T(8,128)(2,1)S(1)}, bf16[80,896]{1,0:T(8,128)(2,1)S(1)}, u32[]{:S(2)}, u32[]{:S(2)}) collective-permute-start(bf16[80,896]{1,0:T(8,128)(2,1)S(1)} %slice.138), channel_id=1, source_target_pairs={{0,2},{2,0},{1,3},{3,1},{4,6},{6,4},{5,7},{7,5},{8,10},{10,8},{9,1... | collective-permute-start | bytes 430088 | tf_op jit(solution)/shard_map/ppermute | solution.py:62
  94.3 1.1 fusion.6
  95.4 1.9 collective-permute-start.7
  97.3 1.4 collective-permute-done.5
  98.8 39.4 %all_gather.3 = bf16[320,896]{1,0:T(8,128)(2,1)S(1)} all-gather(bf16[40,896]{1,0:T(8,128)(2,1)S(1)} %fusion.43), channel_id=1, replica_groups=mesh['ep'=16,'za'=8,'zb'=2,'core'=2] {'za'}, dimensions={0}, use_global_device_ids=true | all-gather | bytes 645120 | tf_op jit(solution)/shard_map/all_gather | solution.py:164
  138.9 1.3 copy.14
  140.2 7.8 %all-to-all-start.2 = ((bf16[64,56,128]{2,1,0:T(8,128)(2,1)}), bf16[64,56,128]{2,1,0:T(8,128)(2,1)S(1)}, u32[]{:S(2)}, u32[]{:S(2)}) async-start(bf16[64,56,128]{2,1,0:T(8,128)(2,1)} %bitcast.18), calls=%async_computation.2 | async-start | bytes 1835008 | tf_op jit(solution)/shard_map/all_to_all | solution.py:168
  148.1 1.5 convolution_add_fusion.2
  149.6 1.3 convolution_add_fusion.3
  150.9 2.0 collective-permute-start.8
  153.0 2.7 %shard_map.102 = (bf16[160,2048]{1,0:T(8,128)(2,1)}, bf16[160,2048]{1,0:T(8,128)(2,1)}) custom-call(s32[1]{0:T(128)} %bitcast.own_ref, bf16[160,4096]{1,0:T(8,128)(2,1)} %weight.1), custom_call_target="tpu_custom_call" | custom-call | tf_op jit(solution)/shard_map/pallas_call | solution.py:52
  155.7 2.4 %collective-permute-start.9 = (bf16[160,2048]{1,0:T(8,128)(2,1)}, bf16[160,2048]{1,0:T(8,128)(2,1)S(1)}, u32[]{:S(2)}, u32[]{:S(2)}) collective-permute-start(bf16[160,2048]{1,0:T(8,128)(2,1)} %get-tuple-element.28), channel_id=1, source_target_pairs={{0,1},{1,0},{2,3},{3,2},{4,5},{5,4},{6,7},{7,6},{8,9},{9,8},{10,11... | collective-permute-start | bytes 1966088 | tf_op jit(solution)/shard_map/ppermute | solution.py:62
  158.7 1.4 collective-permute-done.9
  161.8 1.7 all-to-all-done.2
  163.6 65.4 %reduce-scatter.2.cloned.1.call-done = bf16[1,224,128]{2,1,0:T(8,128)(2,1)} async-done(((bf16[16,224,128]{2,1,0:T(8,128)(2,1)}), bf16[1,224,128]{2,1,0:T(8,128)(2,1)}) %reduce-scatter.2.cloned.1.call-update) | async-done | bytes 57360 | tf_op jit(solution)/shard_map/reduce_scatter | solution.py:153
  229.0 1.7 fusion.3
  (53 shorter events, 5.7 us)
Async XLA Ops:
  8.2 40.1 %all-to-all-start = ((bf16[8,224,128]{2,1,0:T(8,128)(2,1)}), bf16[8,224,128]{2,1,0:T(8,128)(2,1)S(1)}, u32[]{:S(2)}, u32[]{:S(2)}) async-start(bf16[8,224,128]{2,1,0:T(8,128)(2,1)} %broadcast_in_dim.21), calls=%async_computation | async-start | bytes 917504 | tf_op jit(solution)/shard_map/all_to_all | solution.py:93
  50.3 33.4 %all-to-all-start.1 = ((bf16[16,56,1024]{2,1,0:T(8,128)(2,1)}), bf16[16,56,1024]{2,1,0:T(8,128)(2,1)S(1)}, u32[]{:S(2)}, u32[]{:S(2)}) async-start(bf16[16,56,1024]{2,1,0:T(8,128)(2,1)} %bitcast.95), calls=%async_computation.1 | async-start | bytes 3670016 | tf_op jit(solution)/shard_map/all_to_all | solution.py:136
  60.1 8.4 %copy-start.8 = (bf16[2,8,40,128]{3,2,1,0:T(8,128)(2,1)S(1)}, bf16[2,8,40,128]{3,2,1,0:T(8,128)(2,1)}, u32[]{:S(2)}) copy-start(bf16[2,8,40,128]{3,2,1,0:T(8,128)(2,1)} %get-tuple-element.18) | copy-start | bytes 491524
  60.1 10.4 %copy-start.2 = (bf16[2,40,1024]{2,1,0:T(8,128)(2,1)S(1)}, bf16[2,40,1024]{2,1,0:T(8,128)(2,1)}, u32[]{:S(2)}) copy-start(bf16[2,40,1024]{2,1,0:T(8,128)(2,1)} %get-tuple-element.21) | copy-start | bytes 491524
  60.1 15.0 %copy-start.4 = (bf16[8,40,128]{2,1,0:T(8,128)(2,1)S(1)}, bf16[8,40,128]{2,1,0:T(8,128)(2,1)}, u32[]{:S(2)}) copy-start(bf16[8,40,128]{2,1,0:T(8,128)(2,1)} %get-tuple-element.19) | copy-start | bytes 245764
  60.1 10.3 %collective-permute-start.2 = (bf16[2,2,40,1024]{3,2,1,0:T(8,128)(2,1)}, bf16[2,2,40,1024]{3,2,1,0:T(8,128)(2,1)S(1)}, u32[]{:S(2)}, u32[]{:S(2)}) collective-permute-start(bf16[2,2,40,1024]{3,2,1,0:T(8,128)(2,1)} %get-tuple-element.22), channel_id=1, source_target_pairs={{0,1},{1,0},{2,3},{3,2},{4,5},{5,4},{6,7},{7,6},{8,9},{9,8},{10,11... | collective-permute-start | bytes 983048 | tf_op jit(solution)/shard_map/ppermute | solution.py:62
  66.1 21.3 %collective-permute-start.6 = (bf16[2,320,1024]{2,1,0:T(8,128)(2,1)}, bf16[2,320,1024]{2,1,0:T(8,128)(2,1)}, u32[]{:S(2)}, u32[]{:S(2)}) collective-permute-start(bf16[2,320,1024]{2,1,0:T(8,128)(2,1)} %get-tuple-element.24), channel_id=1, source_target_pairs={{0,1},{1,0},{2,3},{3,2},{4,5},{5,4},{6,7},{7,6},{8,9},{9,8},{10,11... | collective-permute-start | bytes 3932168 | tf_op jit(solution)/shard_map/ppermute | solution.py:62
  68.5 6.5 %collective-permute-start = (bf16[2,8,40,128]{3,2,1,0:T(8,128)(2,1)S(1)}, bf16[2,8,40,128]{3,2,1,0:T(8,128)(2,1)S(1)}, u32[]{:S(2)}, u32[]{:S(2)}) collective-permute-start(bf16[2,8,40,128]{3,2,1,0:T(8,128)(2,1)S(1)} %copy-done.8), channel_id=1, source_target_pairs={{0,1},{1,0},{2,3},{3,2},{4,5},{5,4},{6,7},{7,6},{8,9},{9,8},{10,11... | collective-permute-start | bytes 491528 | tf_op jit(solution)/shard_map/ppermute | solution.py:62
  70.5 13.1 %collective-permute-start.3 = (bf16[2,2,40,1024]{3,2,1,0:T(8,128)(2,1)S(1)}, bf16[2,2,40,1024]{3,2,1,0:T(8,128)(2,1)S(1)}, u32[]{:S(2)}, u32[]{:S(2)}) collective-permute-start(bf16[2,2,40,1024]{3,2,1,0:T(8,128)(2,1)S(1)} %pad_maximum_fusion.2), channel_id=1, source_target_pairs={{0,2},{2,0},{1,3},{3,1},{4,6},{6,4},{5,7},{7,5},{8,10},{10,8},{9,1... | collective-permute-start | bytes 983048 | tf_op jit(solution)/shard_map/ppermute | solution.py:62
  75.1 12.2 %copy-start.3 = (bf16[8,40,128]{2,1,0:T(8,128)(2,1)S(1)}, bf16[8,40,128]{2,1,0:T(8,128)(2,1)}, u32[]{:S(2)}) copy-start(bf16[8,40,128]{2,1,0:T(8,128)(2,1)} %get-tuple-element.17) | copy-start | bytes 245764
  75.8 11.5 %collective-permute-start.1 = (bf16[2,8,40,128]{3,2,1,0:T(8,128)(2,1)}, bf16[2,8,40,128]{3,2,1,0:T(8,128)(2,1)S(1)}, u32[]{:S(2)}, u32[]{:S(2)}) collective-permute-start(bf16[2,8,40,128]{3,2,1,0:T(8,128)(2,1)} %pad_maximum_fusion.3), channel_id=1, source_target_pairs={{0,2},{2,0},{1,3},{3,1},{4,6},{6,4},{5,7},{7,5},{8,10},{10,8},{9,1... | collective-permute-start | bytes 491528 | tf_op jit(solution)/shard_map/ppermute | solution.py:62
  85.2 4.4 %copy-start.1 = (bf16[2,40,1024]{2,1,0:T(8,128)(2,1)S(1)}, bf16[2,40,1024]{2,1,0:T(8,128)(2,1)}, u32[]{:S(2)}) copy-start(bf16[2,40,1024]{2,1,0:T(8,128)(2,1)} %get-tuple-element.20) | copy-start | bytes 491524
  85.2 4.4 %collective-permute-start.4 = (f32[160,896]{1,0:T(8,128)}, f32[160,896]{1,0:T(8,128)S(1)}, u32[]{:S(2)}, u32[]{:S(2)}) collective-permute-start(f32[160,896]{1,0:T(8,128)} %fusion.37), channel_id=1, source_target_pairs={{0,1},{1,0},{2,3},{3,2},{4,5},{5,4},{6,7},{7,6},{8,9},{9,8},{10,11... | collective-permute-start | bytes 1720328 | tf_op jit(solution)/shard_map/ppermute | solution.py:62
  89.6 4.7 %copy-start.6 = (bf16[2,320,1024]{2,1,0:T(8,128)(2,1)S(1)}, bf16[2,320,1024]{2,1,0:T(8,128)(2,1)}, u32[]{:S(2)}) copy-start(bf16[2,320,1024]{2,1,0:T(8,128)(2,1)} %get-tuple-element.23) | copy-start | bytes 3932164
  90.4 8.3 %collective-permute-start.5 = (bf16[80,896]{1,0:T(8,128)(2,1)S(1)}, bf16[80,896]{1,0:T(8,128)(2,1)S(1)}, u32[]{:S(2)}, u32[]{:S(2)}) collective-permute-start(bf16[80,896]{1,0:T(8,128)(2,1)S(1)} %slice.138), channel_id=1, source_target_pairs={{0,2},{2,0},{1,3},{3,1},{4,6},{6,4},{5,7},{7,5},{8,10},{10,8},{9,1... | collective-permute-start | bytes 430088 | tf_op jit(solution)/shard_map/ppermute | solution.py:62
  95.4 52.6 %collective-permute-start.7 = (bf16[8,224,128]{2,1,0:T(8,128)(2,1)S(1)}, bf16[8,224,128]{2,1,0:T(8,128)(2,1)S(1)}, u32[]{:S(2)}, u32[]{:S(2)}) collective-permute-start(bf16[8,224,128]{2,1,0:T(8,128)(2,1)S(1)} %all-to-all-done), channel_id=1, source_target_pairs={{0,2},{2,0},{1,3},{3,1},{4,6},{6,4},{5,7},{7,5},{8,10},{10,8},{9,1... | collective-permute-start | bytes 1376264 | tf_op jit(solution)/shard_map/ppermute | solution.py:62
  138.9 9.2 %copy-start.10 = (f32[320,224]{1,0:T(8,128)S(1)}, f32[320,224]{1,0:T(8,128)}, u32[]{:S(2)}) copy-start(f32[320,224]{1,0:T(8,128)} %fusion.4) | copy-start | bytes 860164
  140.2 9.3 %copy-start.7 = (bf16[2,320,1024]{2,1,0:T(8,128)(2,1)S(1)}, bf16[2,320,1024]{2,1,0:T(8,128)(2,1)}, u32[]{:S(2)}) copy-start(bf16[2,320,1024]{2,1,0:T(8,128)(2,1)} %get-tuple-element.23) | copy-start | bytes 3932164
  140.2 23.2 %all-to-all-start.2 = ((bf16[64,56,128]{2,1,0:T(8,128)(2,1)}), bf16[64,56,128]{2,1,0:T(8,128)(2,1)S(1)}, u32[]{:S(2)}, u32[]{:S(2)}) async-start(bf16[64,56,128]{2,1,0:T(8,128)(2,1)} %bitcast.18), calls=%async_computation.2 | async-start | bytes 1835008 | tf_op jit(solution)/shard_map/all_to_all | solution.py:168
  148.0 80.9 %reduce-scatter.2.cloned.1.call-start = ((), (), s32[]{:S(2)}) async-start(), calls=%async_computation.4 | async-start | bytes 974848 | tf_op jit(solution)/shard_map/reduce_scatter | solution.py:153
  150.9 7.2 %collective-permute-start.8 = (f32[2,320,224]{2,1,0:T(8,128)S(1)}, f32[2,320,224]{2,1,0:T(8,128)S(1)}, u32[]{:S(2)}, u32[]{:S(2)}) collective-permute-start(f32[2,320,224]{2,1,0:T(8,128)S(1)} %pad_maximum_fusion), channel_id=1, source_target_pairs={{0,1},{1,0},{2,3},{3,2},{4,5},{5,4},{6,7},{7,6},{8,9},{9,8},{10,11... | collective-permute-start | bytes 1720328 | tf_op jit(solution)/shard_map/ppermute | solution.py:62
  155.7 2.5 %copy-start = (bf16[160,2048]{1,0:T(8,128)(2,1)S(1)}, bf16[160,2048]{1,0:T(8,128)(2,1)}, u32[]{:S(2)}) copy-start(bf16[160,2048]{1,0:T(8,128)(2,1)} %get-tuple-element.27) | copy-start | bytes 1966084
  155.7 4.3 %collective-permute-start.9 = (bf16[160,2048]{1,0:T(8,128)(2,1)}, bf16[160,2048]{1,0:T(8,128)(2,1)S(1)}, u32[]{:S(2)}, u32[]{:S(2)}) collective-permute-start(bf16[160,2048]{1,0:T(8,128)(2,1)} %get-tuple-element.28), channel_id=1, source_target_pairs={{0,1},{1,0},{2,3},{3,2},{4,5},{5,4},{6,7},{7,6},{8,9},{9,8},{10,11... | collective-permute-start | bytes 1966088 | tf_op jit(solution)/shard_map/ppermute | solution.py:62
  160.5 1.2 copy-start.5
  160.5 1.2 copy-start.9
Sparse Core Ops, SparseCore 0:
  161.8 67.1 reduce-scatter.1

commit v4 on v3

--- a/solution.py
+++ b/solution.py
@@ -21,11 +21,12 @@
     for k in range(4):
         for j in range(own_out.shape[0]):
             tile = j * 4 + (own ^ k)
+            row = j * 4 + (own ^ k ^ ((j & 1) ^ own_ref[1]))
             start = pl.multiple_of(tile * LANES, LANES)
             at = slice(j * LANES, (j + 1) * LANES)
             pairs[k][0, :, at] = gate[:, pl.ds(start, LANES)]
             pairs[k][1, :, at] = up[:, pl.ds(start, LANES)]
-            turns[k][j] = down[tile]
+            turns[k][j] = down[row]
 
 
 def dense_kernel(own_ref, gate, up, keep, give):
@@ -55,7 +56,7 @@
         in_specs=[pl.BlockSpec(memory_space=pltpu.SMEM)]
         + [pl.BlockSpec(memory_space=pltpu.VMEM)] * len(weights),
         out_specs=[pl.BlockSpec(memory_space=pltpu.VMEM)] * len(outs),
-    )(own.reshape(1), *weights)
+    )(own.reshape(-1), *weights)
 
 
 def swap(x, axes, size, k):
@@ -99,7 +100,7 @@
     pair, turn = (2, hid, part), (n_za, hid, width)
     gu_own, gu_far, gu_near, turn_own, turn_far, turn_near = split_up(
         expert_kernel,
-        quad,
+        jnp.stack([quad, lax.axis_index("za") & 1]),
         [pair, pair, (2, *pair), turn, turn, (2, *turn)],
         gate_weight[0],
         up_weight[0],
@@ -161,7 +162,10 @@
     gate_up = even[: 2 * hid] + far.astype(jnp.float32)
     hidden = (jax.nn.silu(gate_up[:hid]) * gate_up[hid:]).astype(jnp.bfloat16)
 
-    units = lax.all_gather(hidden, "za", axis=0, tiled=True)
+    rings = [[chip * 2 + ((chip ^ k) & 1) for chip in range(n_za)] for k in range(2)]
+    units = lax.all_gather(
+        hidden, ("za", "core"), axis=0, tiled=True, axis_index_groups=rings
+    )
     outgoing = jnp.einsum("kt,qkf->qtf", units, columns, preferred_element_type=jnp.float32)
     outgoing = outgoing.astype(jnp.bfloat16)
     outgoing = outgoing.reshape(4 * experts, slots, width)

time: 239 us -> 237 us (level)
  the two profiles are of different devices: /device:TPU:2 before, /device:TPU:4 now
where the time goes in v4:
time: 237 us; the launch traced here: 236 us
  waiting for transfers between devices  99.6 us (42%)
  starting transfers between devices  56.2 us (24%)
  blocking collectives  37 us (16%)
  between operations  13.8 us (6%)
  matrix products  13.7 us (6%)
  Pallas kernels  9.02 us (4%)
  local copies, waits for them, and re-layouts  5.08 us (2%)
    reduce_scatter x1, waiting for transfers between devices, per_device(): lax.psum_scatter(jnp.moveaxis(wide, 1, 0), ('za', 'zb'), scatter_dimensio...  65.5 us
    all_gather x1, blocking collectives, per_device(): lax.all_gather(hidden, ('za', 'core'), axis=0, tiled=True, axis_index_gro...  37 us
    ppermute x10, starting transfers between devices, swap(): return lax.ppermute(x, axes, [(i, i ^ k) for i in range(size)])  25.1 us
    all_to_all x1, waiting for transfers between devices, per_device(): lax.all_to_all(jnp.broadcast_to(tokens, (n_za, rows, width)), 'za', split...  24.3 us
    all_to_all x1, starting transfers between devices, per_device(): lax.all_to_all(jnp.broadcast_to(tokens, (n_za, rows, width)), 'za', split...  15.1 us
    dot_general x10, matrix products, dot(): return lax.dot_general(a, b, dims, preferred_element_type=jnp.float32)  13 us
    pallas_call x3, Pallas kernels, split_up(): pl.pallas_call(kernel, out_shape=[jax.ShapeDtypeStruct(shape, jnp.bfloat1...  9.02 us
    ppermute x10, waiting for transfers between devices, swap(): return lax.ppermute(x, axes, [(i, i ^ k) for i in range(size)])  8.64 us
  transfers between devices with their start and end apart: 14, of which 6 were waited for; matrix products, arithmetic and copies ran while one was open for 6% of the time, Pallas kernels for 4%

profile of v4, /device:TPU:4, one launch (start us, length us, event | category | flops | bytes accessed | tf_op | source)
XLA Modules:
  0.0 236.1 jit_solution(18119945725110516442)
XLA Ops:
  6.5 1.6 broadcast_in_dim.21
  8.2 15.1 %all-to-all-start = ((bf16[8,224,128]{2,1,0:T(8,128)(2,1)}), bf16[8,224,128]{2,1,0:T(8,128)(2,1)S(1)}, u32[]{:S(2)}, u32[]{:S(2)}) async-start(bf16[8,224,128]{2,1,0:T(8,128)(2,1)} %broadcast_in_dim.21), calls=%async_computation | async-start | bytes 917504 | tf_op jit(solution)/shard_map/all_to_all | solution.py:94
  24.1 24.3 %all-to-all-done = bf16[8,224,128]{2,1,0:T(8,128)(2,1)S(1)} async-done(((bf16[8,224,128]{2,1,0:T(8,128)(2,1)}), bf16[8,224,128]{2,1,0:T(8,128)(2,1)S(1)}, u32[]{:S(2)}, u32[]{:S(2)}) %all-to-all-start) | async-done | bytes 458784 | tf_op jit(solution)/shard_map/all_to_all | solution.py:94
  48.3 1.9 convolution_convert_fusion
  50.3 7.4 %all-to-all-start.1 = ((bf16[16,56,1024]{2,1,0:T(8,128)(2,1)}), bf16[16,56,1024]{2,1,0:T(8,128)(2,1)S(1)}, u32[]{:S(2)}, u32[]{:S(2)}) async-start(bf16[16,56,1024]{2,1,0:T(8,128)(2,1)} %bitcast.96), calls=%async_computation.1 | async-start | bytes 3670016 | tf_op jit(solution)/shard_map/all_to_all | solution.py:137
  58.3 2.4 shard_map.100
  60.7 2.1 collective-permute-start.2
  62.7 3.9 %shard_map.101 = (bf16[2,320,1024]{2,1,0:T(8,128)(2,1)}, bf16[2,320,1024]{2,1,0:T(8,128)(2,1)}) custom-call(s32[1]{0:T(128)} %bitcast.own_ref, bf16[160,4096]{1,0:T(8,128)(2,1)} %gate.1, bf16[160,4096]{1,0:T(8,128)(2,1)} %up.1), custom_call_target="tpu_custom_call" | custom-call | tf_op jit(solution)/shard_map/pallas_call | solution.py:53
  66.7 2.4 %collective-permute-start.6 = (bf16[2,320,1024]{2,1,0:T(8,128)(2,1)}, bf16[2,320,1024]{2,1,0:T(8,128)(2,1)}, u32[]{:S(2)}, u32[]{:S(2)}) collective-permute-start(bf16[2,320,1024]{2,1,0:T(8,128)(2,1)} %get-tuple-element.24), channel_id=1, source_target_pairs={{0,1},{1,0},{2,3},{3,2},{4,5},{5,4},{6,7},{7,6},{8,9},{9,8},{10,11... | collective-permute-start | bytes 3932168 | tf_op jit(solution)/shard_map/ppermute | solution.py:63
  69.1 1.9 collective-permute-start
  71.1 4.5 %collective-permute-start.3 = (bf16[2,2,40,1024]{3,2,1,0:T(8,128)(2,1)S(1)}, bf16[2,2,40,1024]{3,2,1,0:T(8,128)(2,1)S(1)}, u32[]{:S(2)}, u32[]{:S(2)}) collective-permute-start(bf16[2,2,40,1024]{3,2,1,0:T(8,128)(2,1)S(1)} %pad_maximum_fusion.2), channel_id=1, source_target_pairs={{0,2},{2,0},{1,3},{3,1},{4,6},{6,4},{5,7},{7,5},{8,10},{10,8},{9,1... | collective-permute-start | bytes 983048 | tf_op jit(solution)/shard_map/ppermute | solution.py:63
  76.4 1.9 collective-permute-start.1
  78.3 5.9 %collective-permute-done.3 = bf16[2,2,40,1024]{3,2,1,0:T(8,128)(2,1)S(1)} collective-permute-done((bf16[2,2,40,1024]{3,2,1,0:T(8,128)(2,1)S(1)}, bf16[2,2,40,1024]{3,2,1,0:T(8,128)(2,1)S(1)}, u32[]{:S(2)}, u32[]{:S(2)}) %collective-permute-start.3) | collective-permute-done | bytes 327712 | tf_op jit(solution)/shard_map/ppermute | solution.py:63
  84.2 1.6 fusion.37
  85.8 2.0 collective-permute-start.4
  88.0 2.2 fusion.4
  91.0 3.9 %collective-permute-start.5 = (bf16[80,896]{1,0:T(8,128)(2,1)S(1)}, bf16[80,896]{1,0:T(8,128)(2,1)S(1)}, u32[]{:S(2)}, u32[]{:S(2)}) collective-permute-start(bf16[80,896]{1,0:T(8,128)(2,1)S(1)} %slice.138), channel_id=1, source_target_pairs={{0,2},{2,0},{1,3},{3,1},{4,6},{6,4},{5,7},{7,5},{8,10},{10,8},{9,1... | collective-permute-start | bytes 430088 | tf_op jit(solution)/shard_map/ppermute | solution.py:63
  94.9 1.1 fusion.6
  96.0 1.9 collective-permute-start.7
  97.9 1.4 collective-permute-done.5
  99.4 37.0 %all_gather.3 = bf16[320,896]{1,0:T(8,128)(2,1)S(1)} all-gather(bf16[40,896]{1,0:T(8,128)(2,1)S(1)} %fusion.43), channel_id=1, replica_groups={{0,5,8,13,16,21,24,29},{1,4,9,12,17,20,25,28},{2,7,10,15,18,23,26,31},{..., dimensions={0}, use_global_device_ids=true | all-gather | bytes 645120 | tf_op jit(solution)/shard_map/all_gather | solution.py:166
  137.2 1.3 copy.14
  138.5 8.5 %all-to-all-start.2 = ((bf16[64,56,128]{2,1,0:T(8,128)(2,1)}), bf16[64,56,128]{2,1,0:T(8,128)(2,1)S(1)}, u32[]{:S(2)}, u32[]{:S(2)}) async-start(bf16[64,56,128]{2,1,0:T(8,128)(2,1)} %bitcast.19), calls=%async_computation.2 | async-start | bytes 1835008 | tf_op jit(solution)/shard_map/all_to_all | solution.py:172
  147.1 1.4 convolution_add_fusion.2
  148.5 1.3 convolution_add_fusion.3
  149.9 2.0 collective-permute-start.8
  152.0 2.7 %shard_map.102 = (bf16[160,2048]{1,0:T(8,128)(2,1)}, bf16[160,2048]{1,0:T(8,128)(2,1)}) custom-call(s32[1]{0:T(128)} %bitcast.own_ref, bf16[160,4096]{1,0:T(8,128)(2,1)} %weight.1), custom_call_target="tpu_custom_call" | custom-call | tf_op jit(solution)/shard_map/pallas_call | solution.py:53
  154.7 2.4 %collective-permute-start.9 = (bf16[160,2048]{1,0:T(8,128)(2,1)}, bf16[160,2048]{1,0:T(8,128)(2,1)S(1)}, u32[]{:S(2)}, u32[]{:S(2)}) collective-permute-start(bf16[160,2048]{1,0:T(8,128)(2,1)} %get-tuple-element.28), channel_id=1, source_target_pairs={{0,1},{1,0},{2,3},{3,2},{4,5},{5,4},{6,7},{7,6},{8,9},{9,8},{10,11... | collective-permute-start | bytes 1966088 | tf_op jit(solution)/shard_map/ppermute | solution.py:63
  157.7 1.4 collective-permute-done.9
  160.8 1.2 all-to-all-done.2
  162.1 65.5 %reduce-scatter.2.cloned.1.call-done = bf16[1,224,128]{2,1,0:T(8,128)(2,1)} async-done(((bf16[16,224,128]{2,1,0:T(8,128)(2,1)}), bf16[1,224,128]{2,1,0:T(8,128)(2,1)}) %reduce-scatter.2.cloned.1.call-update) | async-done | bytes 57360 | tf_op jit(solution)/shard_map/reduce_scatter | solution.py:154
  227.6 1.7 fusion.3
  (54 shorter events, 6.2 us)
Async XLA Ops:
  8.2 40.1 %all-to-all-start = ((bf16[8,224,128]{2,1,0:T(8,128)(2,1)}), bf16[8,224,128]{2,1,0:T(8,128)(2,1)S(1)}, u32[]{:S(2)}, u32[]{:S(2)}) async-start(bf16[8,224,128]{2,1,0:T(8,128)(2,1)} %broadcast_in_dim.21), calls=%async_computation | async-start | bytes 917504 | tf_op jit(solution)/shard_map/all_to_all | solution.py:94
  50.3 33.9 %all-to-all-start.1 = ((bf16[16,56,1024]{2,1,0:T(8,128)(2,1)}), bf16[16,56,1024]{2,1,0:T(8,128)(2,1)S(1)}, u32[]{:S(2)}, u32[]{:S(2)}) async-start(bf16[16,56,1024]{2,1,0:T(8,128)(2,1)} %bitcast.96), calls=%async_computation.1 | async-start | bytes 3670016 | tf_op jit(solution)/shard_map/all_to_all | solution.py:137
  60.7 8.4 %copy-start.8 = (bf16[2,8,40,128]{3,2,1,0:T(8,128)(2,1)S(1)}, bf16[2,8,40,128]{3,2,1,0:T(8,128)(2,1)}, u32[]{:S(2)}) copy-start(bf16[2,8,40,128]{3,2,1,0:T(8,128)(2,1)} %get-tuple-element.18) | copy-start | bytes 491524
  60.7 10.4 %copy-start.2 = (bf16[2,40,1024]{2,1,0:T(8,128)(2,1)S(1)}, bf16[2,40,1024]{2,1,0:T(8,128)(2,1)}, u32[]{:S(2)}) copy-start(bf16[2,40,1024]{2,1,0:T(8,128)(2,1)} %get-tuple-element.21) | copy-start | bytes 491524
  60.7 15.0 %copy-start.4 = (bf16[8,40,128]{2,1,0:T(8,128)(2,1)S(1)}, bf16[8,40,128]{2,1,0:T(8,128)(2,1)}, u32[]{:S(2)}) copy-start(bf16[8,40,128]{2,1,0:T(8,128)(2,1)} %get-tuple-element.19) | copy-start | bytes 245764
  60.7 10.3 %collective-permute-start.2 = (bf16[2,2,40,1024]{3,2,1,0:T(8,128)(2,1)}, bf16[2,2,40,1024]{3,2,1,0:T(8,128)(2,1)S(1)}, u32[]{:S(2)}, u32[]{:S(2)}) collective-permute-start(bf16[2,2,40,1024]{3,2,1,0:T(8,128)(2,1)} %get-tuple-element.22), channel_id=1, source_target_pairs={{0,1},{1,0},{2,3},{3,2},{4,5},{5,4},{6,7},{7,6},{8,9},{9,8},{10,11... | collective-permute-start | bytes 983048 | tf_op jit(solution)/shard_map/ppermute | solution.py:63
  66.7 21.3 %collective-permute-start.6 = (bf16[2,320,1024]{2,1,0:T(8,128)(2,1)}, bf16[2,320,1024]{2,1,0:T(8,128)(2,1)}, u32[]{:S(2)}, u32[]{:S(2)}) collective-permute-start(bf16[2,320,1024]{2,1,0:T(8,128)(2,1)} %get-tuple-element.24), channel_id=1, source_target_pairs={{0,1},{1,0},{2,3},{3,2},{4,5},{5,4},{6,7},{7,6},{8,9},{9,8},{10,11... | collective-permute-start | bytes 3932168 | tf_op jit(solution)/shard_map/ppermute | solution.py:63
  69.1 6.5 %collective-permute-start = (bf16[2,8,40,128]{3,2,1,0:T(8,128)(2,1)S(1)}, bf16[2,8,40,128]{3,2,1,0:T(8,128)(2,1)S(1)}, u32[]{:S(2)}, u32[]{:S(2)}) collective-permute-start(bf16[2,8,40,128]{3,2,1,0:T(8,128)(2,1)S(1)} %copy-done.8), channel_id=1, source_target_pairs={{0,1},{1,0},{2,3},{3,2},{4,5},{5,4},{6,7},{7,6},{8,9},{9,8},{10,11... | collective-permute-start | bytes 491528 | tf_op jit(solution)/shard_map/ppermute | solution.py:63
  71.1 13.1 %collective-permute-start.3 = (bf16[2,2,40,1024]{3,2,1,0:T(8,128)(2,1)S(1)}, bf16[2,2,40,1024]{3,2,1,0:T(8,128)(2,1)S(1)}, u32[]{:S(2)}, u32[]{:S(2)}) collective-permute-start(bf16[2,2,40,1024]{3,2,1,0:T(8,128)(2,1)S(1)} %pad_maximum_fusion.2), channel_id=1, source_target_pairs={{0,2},{2,0},{1,3},{3,1},{4,6},{6,4},{5,7},{7,5},{8,10},{10,8},{9,1... | collective-permute-start | bytes 983048 | tf_op jit(solution)/shard_map/ppermute | solution.py:63
  75.7 12.2 %copy-start.3 = (bf16[8,40,128]{2,1,0:T(8,128)(2,1)S(1)}, bf16[8,40,128]{2,1,0:T(8,128)(2,1)}, u32[]{:S(2)}) copy-start(bf16[8,40,128]{2,1,0:T(8,128)(2,1)} %get-tuple-element.17) | copy-start | bytes 245764
  76.4 11.5 %collective-permute-start.1 = (bf16[2,8,40,128]{3,2,1,0:T(8,128)(2,1)}, bf16[2,8,40,128]{3,2,1,0:T(8,128)(2,1)S(1)}, u32[]{:S(2)}, u32[]{:S(2)}) collective-permute-start(bf16[2,8,40,128]{3,2,1,0:T(8,128)(2,1)} %pad_maximum_fusion.3), channel_id=1, source_target_pairs={{0,2},{2,0},{1,3},{3,1},{4,6},{6,4},{5,7},{7,5},{8,10},{10,8},{9,1... | collective-permute-start | bytes 491528 | tf_op jit(solution)/shard_map/ppermute | solution.py:63
  85.8 4.4 %copy-start.1 = (bf16[2,40,1024]{2,1,0:T(8,128)(2,1)S(1)}, bf16[2,40,1024]{2,1,0:T(8,128)(2,1)}, u32[]{:S(2)}) copy-start(bf16[2,40,1024]{2,1,0:T(8,128)(2,1)} %get-tuple-element.20) | copy-start | bytes 491524
  85.8 4.4 %collective-permute-start.4 = (f32[160,896]{1,0:T(8,128)}, f32[160,896]{1,0:T(8,128)S(1)}, u32[]{:S(2)}, u32[]{:S(2)}) collective-permute-start(f32[160,896]{1,0:T(8,128)} %fusion.37), channel_id=1, source_target_pairs={{0,1},{1,0},{2,3},{3,2},{4,5},{5,4},{6,7},{7,6},{8,9},{9,8},{10,11... | collective-permute-start | bytes 1720328 | tf_op jit(solution)/shard_map/ppermute | solution.py:63
  90.2 4.7 %copy-start.6 = (bf16[2,320,1024]{2,1,0:T(8,128)(2,1)S(1)}, bf16[2,320,1024]{2,1,0:T(8,128)(2,1)}, u32[]{:S(2)}) copy-start(bf16[2,320,1024]{2,1,0:T(8,128)(2,1)} %get-tuple-element.23) | copy-start | bytes 3932164
  91.0 8.3 %collective-permute-start.5 = (bf16[80,896]{1,0:T(8,128)(2,1)S(1)}, bf16[80,896]{1,0:T(8,128)(2,1)S(1)}, u32[]{:S(2)}, u32[]{:S(2)}) collective-permute-start(bf16[80,896]{1,0:T(8,128)(2,1)S(1)} %slice.138), channel_id=1, source_target_pairs={{0,2},{2,0},{1,3},{3,1},{4,6},{6,4},{5,7},{7,5},{8,10},{10,8},{9,1... | collective-permute-start | bytes 430088 | tf_op jit(solution)/shard_map/ppermute | solution.py:63
  96.0 51.1 %collective-permute-start.7 = (bf16[8,224,128]{2,1,0:T(8,128)(2,1)S(1)}, bf16[8,224,128]{2,1,0:T(8,128)(2,1)S(1)}, u32[]{:S(2)}, u32[]{:S(2)}) collective-permute-start(bf16[8,224,128]{2,1,0:T(8,128)(2,1)S(1)} %all-to-all-done), channel_id=1, source_target_pairs={{0,2},{2,0},{1,3},{3,1},{4,6},{6,4},{5,7},{7,5},{8,10},{10,8},{9,1... | collective-permute-start | bytes 1376264 | tf_op jit(solution)/shard_map/ppermute | solution.py:63
  137.2 9.9 %copy-start.10 = (f32[320,224]{1,0:T(8,128)S(1)}, f32[320,224]{1,0:T(8,128)}, u32[]{:S(2)}) copy-start(f32[320,224]{1,0:T(8,128)} %fusion.4) | copy-start | bytes 860164
  138.5 10.1 %copy-start.7 = (bf16[2,320,1024]{2,1,0:T(8,128)(2,1)S(1)}, bf16[2,320,1024]{2,1,0:T(8,128)(2,1)}, u32[]{:S(2)}) copy-start(bf16[2,320,1024]{2,1,0:T(8,128)(2,1)} %get-tuple-element.23) | copy-start | bytes 3932164
  138.5 23.5 %all-to-all-start.2 = ((bf16[64,56,128]{2,1,0:T(8,128)(2,1)}), bf16[64,56,128]{2,1,0:T(8,128)(2,1)S(1)}, u32[]{:S(2)}, u32[]{:S(2)}) async-start(bf16[64,56,128]{2,1,0:T(8,128)(2,1)} %bitcast.19), calls=%async_computation.2 | async-start | bytes 1835008 | tf_op jit(solution)/shard_map/all_to_all | solution.py:172
  147.0 80.6 %reduce-scatter.2.cloned.1.call-start = ((), (), s32[]{:S(2)}) async-start(), calls=%async_computation.4 | async-start | bytes 974848 | tf_op jit(solution)/shard_map/reduce_scatter | solution.py:154
  149.9 7.2 %collective-permute-start.8 = (f32[2,320,224]{2,1,0:T(8,128)S(1)}, f32[2,320,224]{2,1,0:T(8,128)S(1)}, u32[]{:S(2)}, u32[]{:S(2)}) collective-permute-start(f32[2,320,224]{2,1,0:T(8,128)S(1)} %pad_maximum_fusion), channel_id=1, source_target_pairs={{0,1},{1,0},{2,3},{3,2},{4,5},{5,4},{6,7},{7,6},{8,9},{9,8},{10,11... | collective-permute-start | bytes 1720328 | tf_op jit(solution)/shard_map/ppermute | solution.py:63
  154.7 2.5 %copy-start = (bf16[160,2048]{1,0:T(8,128)(2,1)S(1)}, bf16[160,2048]{1,0:T(8,128)(2,1)}, u32[]{:S(2)}) copy-start(bf16[160,2048]{1,0:T(8,128)(2,1)} %get-tuple-element.27) | copy-start | bytes 1966084
  154.7 4.3 %collective-permute-start.9 = (bf16[160,2048]{1,0:T(8,128)(2,1)}, bf16[160,2048]{1,0:T(8,128)(2,1)S(1)}, u32[]{:S(2)}, u32[]{:S(2)}) collective-permute-start(bf16[160,2048]{1,0:T(8,128)(2,1)} %get-tuple-element.28), channel_id=1, source_target_pairs={{0,1},{1,0},{2,3},{3,2},{4,5},{5,4},{6,7},{7,6},{8,9},{9,8},{10,11... | collective-permute-start | bytes 1966088 | tf_op jit(solution)/shard_map/ppermute | solution.py:63
  159.5 1.2 copy-start.5
  159.5 1.2 copy-start.9
Sparse Core Ops, SparseCore 0:
  160.8 66.7 reduce-scatter.1

commit v5 on v4

--- a/solution.py
+++ b/solution.py
@@ -144,7 +144,8 @@
     own_part, pair_part = (
         first + dot(w[1], theirs, LAST) for first, w in zip(firsts, (dense_keep, dense_came))
     )
-    came_part = swap(jnp.stack([pair_part, own_part]), "core", 2, 1)
+    outgoing_part = jnp.stack([pair_part, own_part]).astype(jnp.bfloat16)
+    came_part = swap(outgoing_part, "core", 2, 1).astype(jnp.float32)
     dense_hidden = []
     for gu_sum in (own_part + came_part[0], pair_part + came_part[1]):
         value = jax.nn.silu(gu_sum[:dense_hid]) * gu_sum[dense_hid:]
@@ -156,7 +157,7 @@
     )
 
     odd = dot(jnp.concatenate([gu[1], gu[3]], 0), landed, LAST)
-    odd_came = swap(odd, "core", 2, 1)
+    odd_came = swap(odd.astype(jnp.bfloat16), "core", 2, 1).astype(jnp.float32)
     even = dot(jnp.concatenate([gu[0], gu[2]], 0), landed, LAST) + odd_came
     far = swap(even[2 * hid :].astype(jnp.bfloat16), "zb", 2, 1)
     gate_up = even[: 2 * hid] + far.astype(jnp.float32)
@@ -171,12 +172,15 @@
     outgoing = outgoing.reshape(4 * experts, slots, width)
     back = lax.all_to_all(outgoing, ("zb", "core", "ep"), split_axis=0, concat_axis=0, tiled=True)
 
+    gated = jax.nn.sigmoid(branch_gate)[None, :] * dense_out.astype(jnp.float32)
+    gated = lax.optimization_barrier(gated)
     token = lax.broadcasted_iota(jnp.int32, (rows, experts * slots), 0)
     spread = jnp.where(token == chosen[None, :], pick_weights.reshape(1, -1), 0.0)
     parts = back.reshape(4, experts * slots, width).astype(jnp.float32)
     results = jnp.sum(parts, axis=0).astype(jnp.bfloat16)
-    mixture = dot(spread.astype(jnp.bfloat16), results, PLAIN)
-    mixed = mixture + jax.nn.sigmoid(branch_gate)[None, :] * dense_out.astype(jnp.float32)
+    spread = lax.optimization_barrier(spread.astype(jnp.bfloat16))
+    mixture = dot(spread, results, PLAIN)
+    mixed = mixture + gated
     return mixed.astype(jnp.bfloat16)
 
 

time: 237 us -> 238 us (level)
  the two profiles are of different devices: /device:TPU:4 before, /device:TPU:2 now
where the time goes in v5:
time: 238 us; the launch traced here: 237 us
  waiting for transfers between devices  108 us (45%)
  starting transfers between devices  57.1 us (24%)
  blocking collectives  28.5 us (12%)
  between operations  13.8 us (6%)
  matrix products  11.5 us (5%)
  Pallas kernels  9 us (4%)
  local copies, waits for them, and re-layouts  5.05 us (2%)
  other arithmetic  3.45 us (1%)
    reduce_scatter x1, waiting for transfers between devices, per_device(): lax.psum_scatter(jnp.moveaxis(wide, 1, 0), ('za', 'zb'), scatter_dimensio...  68.7 us
    all_gather x1, blocking collectives, per_device(): lax.all_gather(hidden, ('za', 'core'), axis=0, tiled=True, axis_index_gro...  28.5 us
    ppermute x10, starting transfers between devices, swap(): return lax.ppermute(x, axes, [(i, i ^ k) for i in range(size)])  25.2 us
    all_to_all x1, waiting for transfers between devices, per_device(): lax.all_to_all(jnp.broadcast_to(tokens, (n_za, rows, width)), 'za', split...  24.3 us
    all_to_all x1, starting transfers between devices, per_device(): lax.all_to_all(jnp.broadcast_to(tokens, (n_za, rows, width)), 'za', split...  15.1 us
    ppermute x10, waiting for transfers between devices, swap(): return lax.ppermute(x, axes, [(i, i ^ k) for i in range(size)])  15 us
    dot_general x10, matrix products, dot(): return lax.dot_general(a, b, dims, preferred_element_type=jnp.float32)  10.7 us
    all_to_all x1, starting transfers between devices, per_device(): lax.all_to_all(outgoing, ('zb', 'core', 'ep'), split_axis=0, concat_axis=...  9.32 us
  transfers between devices with their start and end apart: 14, of which 7 were waited for; matrix products, arithmetic and copies ran while one was open for 6% of the time, Pallas kernels for 4%

profile of v5, /device:TPU:2, one launch (start us, length us, event | category | flops | bytes accessed | tf_op | source)
XLA Modules:
  0.0 236.5 jit_solution(18437513807314406976)
XLA Ops:
  6.5 1.7 broadcast_in_dim.21
  8.2 15.1 %all-to-all-start = ((bf16[8,224,128]{2,1,0:T(8,128)(2,1)}), bf16[8,224,128]{2,1,0:T(8,128)(2,1)S(1)}, u32[]{:S(2)}, u32[]{:S(2)}) async-start(bf16[8,224,128]{2,1,0:T(8,128)(2,1)} %broadcast_in_dim.21), calls=%async_computation | async-start | bytes 917504 | tf_op jit(solution)/shard_map/all_to_all | solution.py:94
  24.1 24.3 %all-to-all-done = bf16[8,224,128]{2,1,0:T(8,128)(2,1)S(1)} async-done(((bf16[8,224,128]{2,1,0:T(8,128)(2,1)}), bf16[8,224,128]{2,1,0:T(8,128)(2,1)S(1)}, u32[]{:S(2)}, u32[]{:S(2)}) %all-to-all-start) | async-done | bytes 458784 | tf_op jit(solution)/shard_map/all_to_all | solution.py:94
  48.3 1.9 convolution_convert_fusion
  50.3 7.5 %all-to-all-start.1 = ((bf16[16,56,1024]{2,1,0:T(8,128)(2,1)}), bf16[16,56,1024]{2,1,0:T(8,128)(2,1)S(1)}, u32[]{:S(2)}, u32[]{:S(2)}) async-start(bf16[16,56,1024]{2,1,0:T(8,128)(2,1)} %bitcast.99), calls=%async_computation.1 | async-start | bytes 3670016 | tf_op jit(solution)/shard_map/all_to_all | solution.py:137
  58.4 2.3 shard_map.100
  60.7 2.0 collective-permute-start
  62.8 2.5 %collective-permute-start.2 = (bf16[2,2,40,1024]{3,2,1,0:T(8,128)(2,1)}, bf16[2,2,40,1024]{3,2,1,0:T(8,128)(2,1)S(1)}, u32[]{:S(2)}, u32[]{:S(2)}) collective-permute-start(bf16[2,2,40,1024]{3,2,1,0:T(8,128)(2,1)} %get-tuple-element.22), channel_id=1, source_target_pairs={{0,1},{1,0},{2,3},{3,2},{4,5},{5,4},{6,7},{7,6},{8,9},{9,8},{10,11... | collective-permute-start | bytes 983048 | tf_op jit(solution)/shard_map/ppermute | solution.py:63
  65.3 3.9 %shard_map.101 = (bf16[2,320,1024]{2,1,0:T(8,128)(2,1)}, bf16[2,320,1024]{2,1,0:T(8,128)(2,1)}) custom-call(s32[1]{0:T(128)} %bitcast.own_ref, bf16[160,4096]{1,0:T(8,128)(2,1)} %gate.1, bf16[160,4096]{1,0:T(8,128)(2,1)} %up.1), custom_call_target="tpu_custom_call" | custom-call | tf_op jit(solution)/shard_map/pallas_call | solution.py:53
  69.2 1.9 collective-permute-start.6
  71.9 4.5 %collective-permute-start.1 = (bf16[2,8,40,128]{3,2,1,0:T(8,128)(2,1)}, bf16[2,8,40,128]{3,2,1,0:T(8,128)(2,1)S(1)}, u32[]{:S(2)}, u32[]{:S(2)}) collective-permute-start(bf16[2,8,40,128]{3,2,1,0:T(8,128)(2,1)} %pad_maximum_fusion.3), channel_id=1, source_target_pairs={{0,2},{2,0},{1,3},{3,1},{4,6},{6,4},{5,7},{7,5},{8,10},{10,8},{9,1... | collective-permute-start | bytes 491528 | tf_op jit(solution)/shard_map/ppermute | solution.py:63
  77.2 1.9 collective-permute-start.3
  79.1 2.3 collective-permute-done.1
  81.5 7.6 %collective-permute-done.3 = bf16[2,2,40,1024]{3,2,1,0:T(8,128)(2,1)S(1)} collective-permute-done((bf16[2,2,40,1024]{3,2,1,0:T(8,128)(2,1)}, bf16[2,2,40,1024]{3,2,1,0:T(8,128)(2,1)S(1)}, u32[]{:S(2)}, u32[]{:S(2)}) %collective-permute-start.3) | collective-permute-done | bytes 327712 | tf_op jit(solution)/shard_map/ppermute | solution.py:63
  89.1 3.0 %collective-permute-start.7 = (bf16[8,224,128]{2,1,0:T(8,128)(2,1)S(1)}, bf16[8,224,128]{2,1,0:T(8,128)(2,1)}, u32[]{:S(2)}, u32[]{:S(2)}) collective-permute-start(bf16[8,224,128]{2,1,0:T(8,128)(2,1)S(1)} %all-to-all-done), channel_id=1, source_target_pairs={{0,2},{2,0},{1,3},{3,1},{4,6},{6,4},{5,7},{7,5},{8,10},{10,8},{9,1... | collective-permute-start | bytes 1376264 | tf_op jit(solution)/shard_map/ppermute | solution.py:63
  92.9 2.1 collective-permute-start.4
  95.0 2.2 fusion.4
  98.4 2.9 %collective-permute-start.5 = (bf16[80,896]{1,0:T(8,128)(2,1)S(1)}, bf16[80,896]{1,0:T(8,128)(2,1)S(1)}, u32[]{:S(2)}, u32[]{:S(2)}) collective-permute-start(bf16[80,896]{1,0:T(8,128)(2,1)S(1)} %slice.138), channel_id=1, source_target_pairs={{0,2},{2,0},{1,3},{3,1},{4,6},{6,4},{5,7},{7,5},{8,10},{10,8},{9,1... | collective-permute-start | bytes 430088 | tf_op jit(solution)/shard_map/ppermute | solution.py:63
  101.2 1.7 collective-permute-done.7
  102.9 1.4 convolution_add_fusion.3
  104.3 2.1 collective-permute-done.5
  106.5 28.5 %all_gather.3 = bf16[320,896]{1,0:T(8,128)(2,1)S(1)} all-gather(bf16[40,896]{1,0:T(8,128)(2,1)S(1)} %fusion.39), channel_id=1, replica_groups={{0,5,8,13,16,21,24,29},{1,4,9,12,17,20,25,28},{2,7,10,15,18,23,26,31},{..., dimensions={0}, use_global_device_ids=true | all-gather | bytes 645120 | tf_op jit(solution)/shard_map/all_gather | solution.py:167
  135.7 1.3 copy.14
  137.0 9.3 %all-to-all-start.2 = ((bf16[64,56,128]{2,1,0:T(8,128)(2,1)}), bf16[64,56,128]{2,1,0:T(8,128)(2,1)S(1)}, u32[]{:S(2)}, u32[]{:S(2)}) async-start(bf16[64,56,128]{2,1,0:T(8,128)(2,1)} %bitcast.19), calls=%async_computation.2 | async-start | bytes 1835008 | tf_op jit(solution)/shard_map/all_to_all | solution.py:173
  146.4 1.6 convolution_add_fusion.2
  148.1 2.0 collective-permute-start.8
  150.2 2.7 %shard_map.102 = (bf16[160,2048]{1,0:T(8,128)(2,1)}, bf16[160,2048]{1,0:T(8,128)(2,1)}) custom-call(s32[1]{0:T(128)} %bitcast.own_ref, bf16[160,4096]{1,0:T(8,128)(2,1)} %weight.1), custom_call_target="tpu_custom_call" | custom-call | tf_op jit(solution)/shard_map/pallas_call | solution.py:53
  152.9 2.4 %collective-permute-start.9 = (bf16[160,2048]{1,0:T(8,128)(2,1)}, bf16[160,2048]{1,0:T(8,128)(2,1)S(1)}, u32[]{:S(2)}, u32[]{:S(2)}) collective-permute-start(bf16[160,2048]{1,0:T(8,128)(2,1)} %get-tuple-element.28), channel_id=1, source_target_pairs={{0,1},{1,0},{2,3},{3,2},{4,5},{5,4},{6,7},{7,6},{8,9},{9,8},{10,11... | collective-permute-start | bytes 1966088 | tf_op jit(solution)/shard_map/ppermute | solution.py:63
  155.9 1.3 collective-permute-done.9
  157.7 1.1 copy.41
  159.1 68.7 %reduce-scatter.2.cloned.1.call-done = bf16[1,224,128]{2,1,0:T(8,128)(2,1)} async-done(((bf16[16,224,128]{2,1,0:T(8,128)(2,1)}), bf16[1,224,128]{2,1,0:T(8,128)(2,1)}) %reduce-scatter.2.cloned.1.call-update) | async-done | bytes 57360 | tf_op jit(solution)/shard_map/reduce_scatter | solution.py:155
  228.8 0.9 fusion.3
  (54 shorter events, 8.0 us)
Async XLA Ops:
  8.2 40.1 %all-to-all-start = ((bf16[8,224,128]{2,1,0:T(8,128)(2,1)}), bf16[8,224,128]{2,1,0:T(8,128)(2,1)S(1)}, u32[]{:S(2)}, u32[]{:S(2)}) async-start(bf16[8,224,128]{2,1,0:T(8,128)(2,1)} %broadcast_in_dim.21), calls=%async_computation | async-start | bytes 917504 | tf_op jit(solution)/shard_map/all_to_all | solution.py:94
  50.3 41.8 %all-to-all-start.1 = ((bf16[16,56,1024]{2,1,0:T(8,128)(2,1)}), bf16[16,56,1024]{2,1,0:T(8,128)(2,1)S(1)}, u32[]{:S(2)}, u32[]{:S(2)}) async-start(bf16[16,56,1024]{2,1,0:T(8,128)(2,1)} %bitcast.99), calls=%async_computation.1 | async-start | bytes 3670016 | tf_op jit(solution)/shard_map/all_to_all | solution.py:137
  60.7 10.5 %copy-start.4 = (bf16[8,40,128]{2,1,0:T(8,128)(2,1)S(1)}, bf16[8,40,128]{2,1,0:T(8,128)(2,1)}, u32[]{:S(2)}) copy-start(bf16[8,40,128]{2,1,0:T(8,128)(2,1)} %get-tuple-element.19) | copy-start | bytes 245764
  60.7 10.4 %collective-permute-start = (bf16[2,8,40,128]{3,2,1,0:T(8,128)(2,1)}, bf16[2,8,40,128]{3,2,1,0:T(8,128)(2,1)S(1)}, u32[]{:S(2)}, u32[]{:S(2)}) collective-permute-start(bf16[2,8,40,128]{3,2,1,0:T(8,128)(2,1)} %get-tuple-element.18), channel_id=1, source_target_pairs={{0,1},{1,0},{2,3},{3,2},{4,5},{5,4},{6,7},{7,6},{8,9},{9,8},{10,11... | collective-permute-start | bytes 491528 | tf_op jit(solution)/shard_map/ppermute | solution.py:63
  62.8 13.7 %copy-start.2 = (bf16[2,40,1024]{2,1,0:T(8,128)(2,1)S(1)}, bf16[2,40,1024]{2,1,0:T(8,128)(2,1)}, u32[]{:S(2)}) copy-start(bf16[2,40,1024]{2,1,0:T(8,128)(2,1)} %get-tuple-element.21) | copy-start | bytes 491524
  62.8 18.7 %copy-start.3 = (bf16[8,40,128]{2,1,0:T(8,128)(2,1)S(1)}, bf16[8,40,128]{2,1,0:T(8,128)(2,1)}, u32[]{:S(2)}) copy-start(bf16[8,40,128]{2,1,0:T(8,128)(2,1)} %get-tuple-element.17) | copy-start | bytes 245764
  62.8 13.6 %collective-permute-start.2 = (bf16[2,2,40,1024]{3,2,1,0:T(8,128)(2,1)}, bf16[2,2,40,1024]{3,2,1,0:T(8,128)(2,1)S(1)}, u32[]{:S(2)}, u32[]{:S(2)}) collective-permute-start(bf16[2,2,40,1024]{3,2,1,0:T(8,128)(2,1)} %get-tuple-element.22), channel_id=1, source_target_pairs={{0,1},{1,0},{2,3},{3,2},{4,5},{5,4},{6,7},{7,6},{8,9},{9,8},{10,11... | collective-permute-start | bytes 983048 | tf_op jit(solution)/shard_map/ppermute | solution.py:63
  69.2 25.7 %collective-permute-start.6 = (bf16[2,320,1024]{2,1,0:T(8,128)(2,1)}, bf16[2,320,1024]{2,1,0:T(8,128)(2,1)}, u32[]{:S(2)}, u32[]{:S(2)}) collective-permute-start(bf16[2,320,1024]{2,1,0:T(8,128)(2,1)} %get-tuple-element.24), channel_id=1, source_target_pairs={{0,1},{1,0},{2,3},{3,2},{4,5},{5,4},{6,7},{7,6},{8,9},{9,8},{10,11... | collective-permute-start | bytes 3932168 | tf_op jit(solution)/shard_map/ppermute | solution.py:63
  71.9 9.6 %collective-permute-start.1 = (bf16[2,8,40,128]{3,2,1,0:T(8,128)(2,1)}, bf16[2,8,40,128]{3,2,1,0:T(8,128)(2,1)S(1)}, u32[]{:S(2)}, u32[]{:S(2)}) collective-permute-start(bf16[2,8,40,128]{3,2,1,0:T(8,128)(2,1)} %pad_maximum_fusion.3), channel_id=1, source_target_pairs={{0,2},{2,0},{1,3},{3,1},{4,6},{6,4},{5,7},{7,5},{8,10},{10,8},{9,1... | collective-permute-start | bytes 491528 | tf_op jit(solution)/shard_map/ppermute | solution.py:63
  77.2 11.9 %collective-permute-start.3 = (bf16[2,2,40,1024]{3,2,1,0:T(8,128)(2,1)}, bf16[2,2,40,1024]{3,2,1,0:T(8,128)(2,1)S(1)}, u32[]{:S(2)}, u32[]{:S(2)}) collective-permute-start(bf16[2,2,40,1024]{3,2,1,0:T(8,128)(2,1)} %pad_maximum_fusion.1), channel_id=1, source_target_pairs={{0,2},{2,0},{1,3},{3,1},{4,6},{6,4},{5,7},{7,5},{8,10},{10,8},{9,1... | collective-permute-start | bytes 983048 | tf_op jit(solution)/shard_map/ppermute | solution.py:63
  89.1 13.8 %collective-permute-start.7 = (bf16[8,224,128]{2,1,0:T(8,128)(2,1)S(1)}, bf16[8,224,128]{2,1,0:T(8,128)(2,1)}, u32[]{:S(2)}, u32[]{:S(2)}) collective-permute-start(bf16[8,224,128]{2,1,0:T(8,128)(2,1)S(1)} %all-to-all-done), channel_id=1, source_target_pairs={{0,2},{2,0},{1,3},{3,1},{4,6},{6,4},{5,7},{7,5},{8,10},{10,8},{9,1... | collective-permute-start | bytes 1376264 | tf_op jit(solution)/shard_map/ppermute | solution.py:63
  92.1 5.0 %copy-start.6 = (bf16[2,320,1024]{2,1,0:T(8,128)(2,1)S(1)}, bf16[2,320,1024]{2,1,0:T(8,128)(2,1)}, u32[]{:S(2)}) copy-start(bf16[2,320,1024]{2,1,0:T(8,128)(2,1)} %get-tuple-element.23) | copy-start | bytes 3932164
  92.9 4.6 %copy-start.1 = (bf16[2,40,1024]{2,1,0:T(8,128)(2,1)S(1)}, bf16[2,40,1024]{2,1,0:T(8,128)(2,1)}, u32[]{:S(2)}) copy-start(bf16[2,40,1024]{2,1,0:T(8,128)(2,1)} %get-tuple-element.20) | copy-start | bytes 491524
  92.9 4.6 %collective-permute-start.4 = (bf16[160,896]{1,0:T(8,128)(2,1)S(1)}, bf16[160,896]{1,0:T(8,128)(2,1)S(1)}, u32[]{:S(2)}, u32[]{:S(2)}) collective-permute-start(bf16[160,896]{1,0:T(8,128)(2,1)S(1)} %convolution_convert_fusion.2), channel_id=1, source_target_pairs={{0,1},{1,0},{2,3},{3,2},{4,5},{5,4},{6,7},{7,6},{8,9},{9,8},{10,11... | collective-permute-start | bytes 860168 | tf_op jit(solution)/shard_map/ppermute | solution.py:63
  98.4 8.1 %collective-permute-start.5 = (bf16[80,896]{1,0:T(8,128)(2,1)S(1)}, bf16[80,896]{1,0:T(8,128)(2,1)S(1)}, u32[]{:S(2)}, u32[]{:S(2)}) collective-permute-start(bf16[80,896]{1,0:T(8,128)(2,1)S(1)} %slice.138), channel_id=1, source_target_pairs={{0,2},{2,0},{1,3},{3,1},{4,6},{6,4},{5,7},{7,5},{8,10},{10,8},{9,1... | collective-permute-start | bytes 430088 | tf_op jit(solution)/shard_map/ppermute | solution.py:63
  135.7 10.7 %copy-start.8 = (f32[320,224]{1,0:T(8,128)S(1)}, f32[320,224]{1,0:T(8,128)}, u32[]{:S(2)}) copy-start(f32[320,224]{1,0:T(8,128)} %fusion.4) | copy-start | bytes 860164
  137.0 91.6 %all-to-all-start.2 = ((bf16[64,56,128]{2,1,0:T(8,128)(2,1)}), bf16[64,56,128]{2,1,0:T(8,128)(2,1)S(1)}, u32[]{:S(2)}, u32[]{:S(2)}) async-start(bf16[64,56,128]{2,1,0:T(8,128)(2,1)} %bitcast.19), calls=%async_computation.2 | async-start | bytes 1835008 | tf_op jit(solution)/shard_map/all_to_all | solution.py:173
  146.4 81.4 %reduce-scatter.2.cloned.1.call-start = ((), (), s32[]{:S(2)}) async-start(), calls=%async_computation.4 | async-start | bytes 974848 | tf_op jit(solution)/shard_map/reduce_scatter | solution.py:155
  148.1 7.2 %collective-permute-start.8 = (bf16[2,320,224]{2,1,0:T(8,128)(2,1)S(1)}, bf16[2,320,224]{2,1,0:T(8,128)(2,1)S(1)}, u32[]{:S(2)}, u32[]{:S(2)}) collective-permute-start(bf16[2,320,224]{2,1,0:T(8,128)(2,1)S(1)} %pad_maximum_fusion.2), channel_id=1, source_target_pairs={{0,1},{1,0},{2,3},{3,2},{4,5},{5,4},{6,7},{7,6},{8,9},{9,8},{10,11... | collective-permute-start | bytes 860168 | tf_op jit(solution)/shard_map/ppermute | solution.py:63
  152.9 2.6 %copy-start = (bf16[160,2048]{1,0:T(8,128)(2,1)S(1)}, bf16[160,2048]{1,0:T(8,128)(2,1)}, u32[]{:S(2)}) copy-start(bf16[160,2048]{1,0:T(8,128)(2,1)} %get-tuple-element.27) | copy-start | bytes 1966084
  152.9 4.3 %collective-permute-start.9 = (bf16[160,2048]{1,0:T(8,128)(2,1)}, bf16[160,2048]{1,0:T(8,128)(2,1)S(1)}, u32[]{:S(2)}, u32[]{:S(2)}) collective-permute-start(bf16[160,2048]{1,0:T(8,128)(2,1)} %get-tuple-element.28), channel_id=1, source_target_pairs={{0,1},{1,0},{2,3},{3,2},{4,5},{5,4},{6,7},{7,6},{8,9},{9,8},{10,11... | collective-permute-start | bytes 1966088 | tf_op jit(solution)/shard_map/ppermute | solution.py:63
  157.7 1.1 copy-start.5
  157.7 1.3 copy-start.7
Sparse Core Ops, SparseCore 0:
  158.9 68.7 reduce-scatter.1
